TPU v7x, 32 devices: a whole 2x2x4 slice. The times are simulated.
32 devices in a mesh: grp: 1, ep: 32 (over z, y, x, core).
Axes of the slice: x: 2, y: 2, z: 4, core: 2. Of those that a mesh axis runs over, the one named last changes fastest.
Arguments:
- residual_input: bfloat16 [768, 2048], P(('grp', 'ep')), may hold values from -6 to 6
- attention_norm_gain: bfloat16 [2048], replicated, may hold values from 0.099609375 to 1.8984375
- receptance_weight: bfloat16 [2048, 1024], P(None, 'ep'), may hold values from -0.125 to 0.125
- key_weight: bfloat16 [2048, 1024], P(None, 'ep'), may hold values from -0.125 to 0.125
- value_weight: bfloat16 [2048, 1024], P(None, 'ep'), may hold values from -0.125 to 0.125
- decay_weight: bfloat16 [2048, 1024], P(None, 'ep'), may hold values from -0.125 to 0.125
- correction_rate_weight: bfloat16 [2048, 1024], P(None, 'ep'), may hold values from -0.125 to 0.125
- output_gate_weight: bfloat16 [2048, 1024], P(None, 'ep'), may hold values from -0.125 to 0.125
- decay_offset: float32 [1024], replicated, may hold values from -3 to 1
- correction_rate_offset: float32 [1024], replicated, may hold values from -1.5 to 1.5
- self_term_weight: float32 [1024], replicated, may hold values from -2 to 2
- head_read_gain: float32 [1024], replicated, may hold values from 0.1 to 1.9
- previous_state: float32 [768, 16, 4096], P(('grp', 'ep')), may hold values from -4 to 4
- attention_output_weight: bfloat16 [1024, 2048], replicated, may hold values from -0.1875 to 0.1875
- feedforward_norm_gain: bfloat16 [2048], replicated, may hold values from 0.099609375 to 1.8984375
- routes: int32 [768, 4], P('grp'), may hold values from 0 to 31, all different within a row; in each aligned block of 24 rows (0 to 23, 24 to 47, ...) at most 4 rows name the same one
- routing_weight: float32 [768, 4], P('grp'), may hold values from 0.2 to 1
- routed_gate_weight: bfloat16 [32, 2048, 512], P('ep'), may hold values from -0.125 to 0.125
- routed_up_weight: bfloat16 [32, 2048, 512], P('ep'), may hold values from -0.125 to 0.125
- routed_down_weight: bfloat16 [32, 512, 2048], P('ep'), may hold values from -0.25 to 0.25
- common_gate_weight: bfloat16 [2048, 512], replicated, may hold values from -0.125 to 0.125
- common_up_weight: bfloat16 [2048, 512], replicated, may hold values from -0.125 to 0.125
- common_down_weight: bfloat16 [512, 2048], replicated, may hold values from -0.25 to 0.25
Outputs:
- hidden_out: bfloat16 [768, 2048], P(('grp', 'ep'))
- next_state: float32 [768, 16, 4096], P(('grp', 'ep'))
Inputs may be any that keep to these rules, and one draw needn't show every extreme that they name: `routes`: the 4 entries of a row differ. In each aligned block of 24 rows (the tokens of one index of ep) no expert is named by more than 4 rows, a bound that some block reaches.
All inputs are finite; a program needn't handle non-finite values.
Results may differ from a plain program's by a relative error of at most 0.013.
Values may be sent and summed in bfloat16 or wider, within the bound.
A program may use at most 128 MiB of HBM per device.

v0:
```python
import functools
import math

import jax
import jax.numpy as jnp
import numpy as np
from jax import lax
from jax.experimental import pallas as pl
from jax.experimental.pallas import tpu as pltpu
from jax.sharding import PartitionSpec as P

HEAD_COUNT = 16
HEAD_SIZE = 64
CAP = 4
ROLES = 6
LANES = 128
F32 = jnp.float32
BF16 = jnp.bfloat16


def rms_norm(value_rows, gain):
    scale = lax.rsqrt(jnp.mean(value_rows * value_rows, axis=-1, keepdims=True) + 1e-06)
    return (value_rows * scale * gain.astype(F32)).astype(BF16)


def expert_mlp(rows, gate_w, up_w, down_w):
    gate = jnp.dot(rows, gate_w, preferred_element_type=F32)
    upward = jnp.dot(rows, up_w, preferred_element_type=F32)
    hidden = (jax.nn.silu(gate) * upward).astype(BF16)
    return jnp.dot(hidden, down_w, preferred_element_type=F32).astype(BF16)


def place_matrices(pieces):
    width = HEAD_SIZE // pieces
    place = np.zeros((pieces, ROLES * width, ROLES * LANES), np.float32)
    for piece in range(pieces):
        for role in range(ROLES):
            for column in range(width):
                for copy in range(LANES // HEAD_SIZE):
                    lane = role * LANES + copy * HEAD_SIZE + piece * width + column
                    place[piece, role * width + column, lane] = 1.0
    return place


def split(value):
    high = value.astype(BF16)
    return high, (value - high.astype(F32)).astype(BF16)


def dot(a, b):
    return jnp.dot(a, b, preferred_element_type=F32)


def mixer_kernel(
    land_ref, place_ref, spread_ref, gather_ref, block_ref, const0, const1, const2, const3, state_ref, out_w_ref,
    resid_ref, gain_ref, select_ref,
    next_ref, middle_ref, normed_ref, rows_ref,
    role_ref, mixed_ref, consts_ref,
):
    step = pl.program_id(0)
    tokens = land_ref.shape[1]
    pieces = place_ref.shape[0]
    step_rows = state_ref.shape[0] * HEAD_COUNT

    @pl.when(step == 0)
    def _():
        for number, source in enumerate((const0, const1, const2, const3)):
            pair = source[...]
            turned = pltpu.roll(pair, HEAD_SIZE, 1)
            first = lax.broadcasted_iota(jnp.int32, pair.shape, 1) < HEAD_SIZE
            count = pair.shape[0]
            consts_ref[number, pl.ds(0, count, stride=2), :] = jnp.where(first, pair, turned)
            consts_ref[number, pl.ds(1, count, stride=2), :] = jnp.where(first, turned, pair)
        for head in range(HEAD_COUNT):
            total = dot(land_ref[head * pieces], place_ref[0])
            for piece in range(1, pieces):
                total = total + dot(land_ref[head * pieces + piece], place_ref[piece])
            for number in range(ROLES):
                part = total[:, number * LANES : (number + 1) * LANES]
                role_ref[number, pl.ds(head, tokens, stride=HEAD_COUNT), :] = part

    base = pl.multiple_of(step * step_rows, step_rows)

    def role(number):
        return role_ref[number, pl.ds(base, step_rows), :]

    def const(number):
        one = consts_ref[number]
        return jnp.concatenate([one] * state_ref.shape[0], axis=0)

    half = HEAD_SIZE / LANES

    def head_sum(value):
        return jnp.sum(value, axis=-1, keepdims=True) * half

    receptance, keys, values = role(0), role(1), role(2)
    decay = jnp.exp(-math.exp(-0.5) * jax.nn.sigmoid(const(0) + role(3)))
    rate = jax.nn.sigmoid(const(1) + role(4))
    unit_key = keys * lax.rsqrt(1.0 + head_sum(keys * keys))
    scaled_key = keys * rate
    removal = unit_key * rate
    self_sum = head_sum(receptance * scaled_key * const(2))

    def twice(value):
        return jnp.concatenate([value, value], axis=1)

    unit_key2, decay2, removal2 = twice(unit_key), twice(decay), twice(removal)
    scaled_key2, receptance2 = twice(scaled_key), twice(receptance)
    values_b = values[:, :HEAD_SIZE].astype(BF16)
    block = block_ref[...]
    chunk = block.shape[0]
    read = jnp.zeros((step_rows, LANES), F32)
    group = state_ref.shape[0]
    for c in range(HEAD_SIZE * HEAD_SIZE // chunk):
        cols = slice(c * chunk, (c + 1) * chunk)
        state = state_ref[:, :, cols].reshape(step_rows, chunk)
        high, low = split(state * unit_key2)
        recalled = dot(high, block) + dot(low, block)
        spread = dot(values_b, spread_ref[:, cols])
        new = state * decay2 - recalled * removal2 + spread * scaled_key2
        next_ref[:, :, cols] = new.reshape(group, HEAD_COUNT, chunk)
        high, low = split(new * receptance2)
        pick = gather_ref[cols, :]
        read = read + dot(high, pick) + dot(low, pick)
    centered = read - head_sum(read) * (1.0 / HEAD_SIZE)
    variance = head_sum(centered * centered) * (1.0 / HEAD_SIZE)
    normal = centered * lax.rsqrt(variance + 0.00064) * const(3)
    mixed_ref[pl.ds(base, step_rows), :] = (normal + self_sum * values) * jax.nn.sigmoid(role(5))

    @pl.when(step == pl.num_programs(0) - 1)
    def _():
        lane = lax.broadcasted_iota(jnp.int32, (tokens, LANES), 1)
        per = LANES // HEAD_SIZE
        parts = []
        for first in range(0, HEAD_COUNT, per):
            part = mixed_ref[pl.ds(first, tokens, stride=HEAD_COUNT), :]
            for other in range(1, per):
                rest = mixed_ref[pl.ds(first + other, tokens, stride=HEAD_COUNT), :]
                part = jnp.where(lane < other * HEAD_SIZE, part, rest)
            parts.append(part.astype(BF16))
        mixed = jnp.concatenate(parts, axis=1)
        attended = dot(mixed, out_w_ref[...]).astype(BF16).astype(F32)
        middle = resid_ref[...].astype(F32) + attended
        middle_ref[...] = middle
        normed = rms_norm(middle, gain_ref[...])
        normed_ref[...] = normed
        rows_ref[...] = dot(select_ref[...], normed).reshape(rows_ref.shape).astype(BF16)


def mixer(land, consts, state, out_w, resid, gain, select):
    sources, tokens, width = land.shape
    pieces = sources // HEAD_COUNT
    model = resid.shape[1]
    group = 8 if tokens % 8 == 0 else 1
    chunk = 4 * HEAD_SIZE
    place = jnp.asarray(place_matrices(pieces), BF16)
    eye = np.eye(HEAD_SIZE, dtype=np.float32)
    spread = jnp.asarray(np.repeat(eye, HEAD_SIZE, axis=1), BF16)
    gather = jnp.asarray(np.repeat(np.concatenate([eye] * (LANES // HEAD_SIZE), 1), HEAD_SIZE, 0), BF16)
    block = jnp.asarray(np.kron(np.eye(chunk // HEAD_SIZE), np.ones((HEAD_SIZE, HEAD_SIZE))), BF16)
    full = lambda array: pl.BlockSpec(array.shape, lambda i: (0,) * array.ndim)
    state_spec = pl.BlockSpec((group,) + state.shape[1:], lambda i: (i, 0, 0))
    operands = (land, place, spread, gather, block, *consts, state, out_w, resid, gain, select)
    specs = [full(a) for a in operands]
    specs[9] = state_spec
    whole = lambda shape: pl.BlockSpec(shape, lambda i: (0,) * len(shape))
    slots = select.shape[0]
    return pl.pallas_call(
        mixer_kernel,
        grid=(tokens // group,),
        out_shape=(
            jax.ShapeDtypeStruct(state.shape, F32),
            jax.ShapeDtypeStruct((tokens, model), F32),
            jax.ShapeDtypeStruct((tokens, model), BF16),
            jax.ShapeDtypeStruct((slots // CAP, CAP, model), BF16),
        ),
        in_specs=specs,
        out_specs=(state_spec, whole((tokens, model)), whole((tokens, model)), whole((slots // CAP, CAP, model))),
        scratch_shapes=[
            pltpu.VMEM((ROLES, tokens * HEAD_COUNT, LANES), F32),
            pltpu.VMEM((tokens * HEAD_COUNT, LANES), F32),
            pltpu.VMEM((4, HEAD_COUNT, LANES), F32),
        ],
        compiler_params=pltpu.CompilerParams(vmem_limit_bytes=50 * 1024 * 1024),
        cost_estimate=pl.CostEstimate(flops=4_000_000_000, bytes_accessed=20_000_000, transcendentals=0),
    )(*operands)


PLANE = 8


def project_kernel(
    depth, normed_ref, w0, w1, w2, w3, w4, w5, land_out,
    weight_ref, held, cols, land,
    z_send, z_recv, near_send, near_recv, half_send, half_recv, core_send, core_recv,
    out_send, out_recv,
):
    total = depth * PLANE
    tokens, model = normed_ref.shape
    cut = model // 2
    me = lax.axis_index("ep")
    core = lax.rem(me, 2)
    x = lax.rem(me // 2, 2)
    y = lax.rem(me // 4, 2)
    along_x = me + 2 - 4 * x
    along_y = me + 4 - 8 * y
    mate = me + 1 - 2 * core
    plane = lax.rem(me, PLANE)
    plane_x, plane_y, plane_c = lax.rem(along_x, PLANE), lax.rem(along_y, PLANE), lax.rem(mate, PLANE)
    far = lax.rem(along_x + 4 - 8 * y, PLANE)
    level = me // PLANE

    def send(source, target, device, send_sem, recv_sem):
        copy = pltpu.make_async_remote_copy(
            src_ref=source, dst_ref=target, send_sem=send_sem, recv_sem=recv_sem,
            device_id={"ep": device}, device_id_type=pl.DeviceIdType.MESH,
        )
        copy.start()
        return copy

    def slot(of_plane, d):
        return held.at[of_plane, lax.rem(level + depth - d, depth)]

    sent = []
    along_z = [None]
    for d in range(1, depth):
        there = lax.rem(me + PLANE * d, total)
        along_z.append(send(normed_ref, slot(plane, 0), there, z_send.at[d], z_recv.at[d]))
    by_y, by_x, by_core = [], [], [[], [], [], []]
    for d in range(depth):
        if d:
            along_z[d].wait_recv()
        source = normed_ref if d == 0 else slot(plane, d)
        here = slot(plane, d)
        by_y.append(send(source, here, along_y, near_send.at[0, d], near_recv.at[0, d]))
        by_x.append(send(source, here, along_x, near_send.at[1, d], near_recv.at[1, d]))
        by_core[0].append(send(source, here, mate, core_send.at[0, d], core_recv.at[0, d]))
        if d == 0:
            held[plane, level] = normed_ref[...]
            weight_ref[...] = jnp.concatenate(
                [w[...] for w in (w0, w1, w2, w3, w4, w5)], axis=0
            )

    def compute(group):
        rows = held[group].astype(F32).reshape(depth * tokens, model).astype(BF16)
        result = lax.dot_general(
            rows, weight_ref[...], (((1,), (1,)), ((), ())), preferred_element_type=F32
        )
        cols[group] = result.reshape(depth, tokens, result.shape[-1]).astype(BF16)

    def give(group):
        for z in range(depth):
            to = z * PLANE + group
            number = lax.rem(to - me + total, total)

            @pl.when(to != me)
            def _():
                send(cols.at[group, z], land.at[me], to, out_send.at[number], out_recv.at[number])

            @pl.when(to == me)
            def _():
                land[me] = cols[group, z]

    compute(plane)
    halves = []
    for d in range(depth):
        by_y[d].wait_recv()
        block = held.at[plane_y, lax.rem(level + depth - d, depth)]
        first = block.at[:, :cut]
        halves.append(send(first, first, along_x, half_send.at[0, d], half_recv.at[0, d]))
        by_core[1].append(send(block, block, mate, core_send.at[1, d], core_recv.at[1, d]))
        by_x[d].wait_recv()
        block = held.at[plane_x, lax.rem(level + depth - d, depth)]
        second = block.at[:, cut:]
        halves.append(send(second, second, along_y, half_send.at[1, d], half_recv.at[1, d]))
        by_core[2].append(send(block, block, mate, core_send.at[2, d], core_recv.at[2, d]))
    compute(plane_y)
    give(plane)
    compute(plane_x)
    give(plane_y)
    for d in range(depth):
        halves[2 * d].wait_recv()
        halves[2 * d + 1].wait_recv()
        block = slot(far, d)
        by_core[3].append(send(block, block, mate, core_send.at[3, d], core_recv.at[3, d]))
    before = plane_x
    compute(far)
    give(before)
    before = far
    for which, group in enumerate((plane, plane_y, plane_x, far)):
        for d in range(depth):
            by_core[which][d].wait_recv()
        other = group + 1 - 2 * core
        compute(other)
        give(before)
        before = other
    give(before)
    for copy in along_z[1:] + by_y + by_x + halves + by_core[0] + by_core[1] + by_core[2] + by_core[3]:
        copy.wait_send()

    def finish(number, carry):
        copy = pltpu.make_async_remote_copy(
            src_ref=cols.at[0, 0], dst_ref=land.at[0],
            send_sem=out_send.at[number], recv_sem=out_recv.at[number],
            device_id={"ep": lax.rem(me + number, total)}, device_id_type=pl.DeviceIdType.MESH,
        )
        copy.wait_recv()
        copy.wait_send()
        return carry

    lax.fori_loop(1, total, finish, 0)
    land_out[...] = land[...]


def project(normed, weights, ep_size):
    depth = ep_size // PLANE
    tokens, model = normed.shape
    weights = [w.T for w in weights]
    width = sum(w.shape[0] for w in weights)
    dma = pltpu.SemaphoreType.DMA
    return pl.pallas_call(
        functools.partial(project_kernel, depth),
        out_shape=jax.ShapeDtypeStruct((ep_size, tokens, width), BF16),
        in_specs=[pl.BlockSpec(memory_space=pltpu.VMEM)] * 7,
        out_specs=pl.BlockSpec(memory_space=pltpu.VMEM),
        scratch_shapes=[
            pltpu.VMEM((width, model), BF16),
            pltpu.VMEM((PLANE, depth, tokens, model), BF16),
            pltpu.VMEM((PLANE, depth, tokens, width), BF16),
            pltpu.VMEM((ep_size, tokens, width), BF16),
            dma((depth,)), dma((depth,)),
            dma((2, depth)), dma((2, depth)),
            dma((2, depth)), dma((2, depth)),
            dma((4, depth)), dma((4, depth)),
            dma((ep_size,)), dma((ep_size,)),
        ],
        compiler_params=pltpu.CompilerParams(
            has_side_effects=True, vmem_limit_bytes=40 * 1024 * 1024
        ),
        cost_estimate=pl.CostEstimate(flops=600_000_000, bytes_accessed=100_000_000, transcendentals=0),
    )(normed, *weights)


def experts_kernel(
    depth, rows_ref, normed_ref, middle_ref, coef_ref, g0, g1, g2, g3, g4, g5, out_ref,
    b0, b1, b2, b3, b4, b5, served, output, returned,
    load_sem, go_send, go_recv, back_send, back_recv,
):
    total = depth * PLANE
    tokens, model = normed_ref.shape
    me = lax.axis_index("ep")
    level = me // PLANE

    def copy_of(source, target, device, send_sem, recv_sem):
        return pltpu.make_async_remote_copy(
            src_ref=source, dst_ref=target, send_sem=send_sem, recv_sem=recv_sem,
            device_id={"ep": device}, device_id_type=pl.DeviceIdType.MESH,
        )

    def go(number):
        to = lax.rem(me + number, total)
        return copy_of(rows_ref.at[to], served.at[me], to, go_send.at[number], go_recv.at[number])

    def back(to):
        number = lax.rem(to - me + total, total)
        return copy_of(
            output.at[to], returned.at[me], to, back_send.at[number], back_recv.at[number]
        )

    def launch(number, carry):
        go(number).start()
        return carry

    lax.fori_loop(1, total, launch, 0)
    loads = [
        pltpu.make_async_copy(source, target, load_sem.at[i])
        for i, (source, target) in enumerate(zip((g0, g1, g2, g3, g4, g5), (b0, b1, b2, b3, b4, b5)))
    ]
    for load in loads:
        load.start()
    served[me] = rows_ref[me]
    for load in loads[:3]:
        load.wait()
    shared = expert_mlp(normed_ref[...], b0[...], b1[...], b2[...])
    partial = middle_ref[...] + shared.astype(F32)
    for load in loads[3:]:
        load.wait()

    for d in range(depth):
        first = lax.rem(level + depth - d, depth) * PLANE

        def arrive(i, carry):
            source = first + i

            @pl.when(source != me)
            def _():
                go(lax.rem(me - source + total, total)).wait_recv()

            return carry

        lax.fori_loop(0, PLANE, arrive, 0)
        rows = served[pl.ds(first, PLANE)].reshape(PLANE * CAP, model)
        result = expert_mlp(rows, b3[...], b4[...], b5[...])
        output[pl.ds(first, PLANE)] = result.reshape(PLANE, CAP, model)

        def give(i, carry):
            source = first + i

            @pl.when(source != me)
            def _():
                back(source).start()

            return carry

        lax.fori_loop(0, PLANE, give, 0)
    returned[me] = output[me]

    def finish(number, carry):
        go(number).wait_send()
        ended = back(lax.rem(me + number, total))
        ended.wait_recv()
        ended.wait_send()
        return carry

    lax.fori_loop(1, total, finish, 0)
    routed = dot(coef_ref[...], returned[...].reshape(total * CAP, model))
    out_ref[...] = (partial + (routed[:tokens] + routed[tokens:])).astype(BF16)


def experts_step(rows, normed, middle, coef, weights, ep_size):
    depth = ep_size // PLANE
    tokens, model = normed.shape
    dma = pltpu.SemaphoreType.DMA
    vmem = pl.BlockSpec(memory_space=pltpu.VMEM)
    return pl.pallas_call(
        functools.partial(experts_kernel, depth),
        out_shape=jax.ShapeDtypeStruct((tokens, model), BF16),
        in_specs=[vmem] * 4 + [pl.BlockSpec(memory_space=pl.ANY)] * 6,
        out_specs=vmem,
        scratch_shapes=[pltpu.VMEM(w.shape, BF16) for w in weights]
        + [pltpu.VMEM(rows.shape, BF16)] * 3
        + [dma((6,))]
        + [dma((ep_size,))] * 4,
        compiler_params=pltpu.CompilerParams(
            has_side_effects=True, vmem_limit_bytes=40 * 1024 * 1024
        ),
        cost_estimate=pl.CostEstimate(flops=1_000_000_000, bytes_accessed=60_000_000, transcendentals=0),
    )(rows, normed, middle, coef, *weights)


def per_device(
    residual_input,
    attention_norm_gain,
    receptance_weight,
    key_weight,
    value_weight,
    decay_weight,
    correction_rate_weight,
    output_gate_weight,
    decay_offset,
    correction_rate_offset,
    self_term_weight,
    head_read_gain,
    previous_state,
    attention_output_weight,
    feedforward_norm_gain,
    routes,
    routing_weight,
    routed_gate_weight,
    routed_up_weight,
    routed_down_weight,
    common_gate_weight,
    common_up_weight,
    common_down_weight,
):
    ep_size = lax.axis_size("ep")
    device = lax.axis_index("ep")
    tokens, model = residual_input.shape
    normed = rms_norm(residual_input.astype(F32), attention_norm_gain)
    own_routes = lax.dynamic_slice_in_dim(routes, device * tokens, tokens, 0)
    own_weight = lax.dynamic_slice_in_dim(routing_weight, device * tokens, tokens, 0)
    experts = routed_gate_weight.shape[0] * ep_size
    match = own_routes[:, :, None] == jnp.arange(experts, dtype=jnp.int32)
    hit = jnp.any(match, axis=1)
    weight = jnp.sum(jnp.where(match, own_weight[:, :, None], 0.0), axis=1)
    rank = jnp.cumsum(hit.astype(jnp.int32), axis=0) - hit.astype(jnp.int32)
    chosen = hit[:, :, None] & (rank[:, :, None] == jnp.arange(CAP, dtype=jnp.int32))
    select = chosen.astype(BF16).reshape(tokens, experts * CAP)
    coefficient = jnp.where(chosen, weight[:, :, None], 0.0).reshape(tokens, experts * CAP)
    coef_high, coef_low = split(coefficient)

    land = project(
        normed,
        (
            receptance_weight,
            key_weight,
            value_weight,
            decay_weight,
            correction_rate_weight,
            output_gate_weight,
        ),
        ep_size,
    )
    consts = [
        c.reshape(-1, LANES)
        for c in (decay_offset, correction_rate_offset, self_term_weight, head_read_gain)
    ]
    next_state, middle, normed_ffn, rows = mixer(
        land,
        consts,
        previous_state,
        attention_output_weight,
        residual_input,
        feedforward_norm_gain.reshape(1, model),
        select.T,
    )
    hidden_out = experts_step(
        rows,
        normed_ffn,
        middle,
        jnp.concatenate((coef_high, coef_low), axis=0),
        (
            common_gate_weight,
            common_up_weight,
            common_down_weight,
            routed_gate_weight[0],
            routed_up_weight[0],
            routed_down_weight[0],
        ),
        ep_size,
    )
    return (hidden_out, next_state)


def solution(mesh):
    return jax.shard_map(
        per_device,
        mesh=mesh,
        in_specs=(
            P(("grp", "ep"), None),
            P(),
            P(None, "ep"),
            P(None, "ep"),
            P(None, "ep"),
            P(None, "ep"),
            P(None, "ep"),
            P(None, "ep"),
            P(),
            P(),
            P(),
            P(),
            P(("grp", "ep"), None, None),
            P(),
            P(),
            P("grp", None),
            P("grp", None),
            P("ep", None, None),
            P("ep", None, None),
            P("ep", None, None),
            P(),
            P(),
            P(),
        ),
        out_specs=(P(("grp", "ep"), None), P(("grp", "ep"), None, None)),
        check_vma=False,
    )
```

profile of v0, /device:TPU:0, one launch (start us, length us, event | category | flops | bytes accessed | tf_op | source)
XLA Modules:
  0.0 107.5 jit_solution(5959397097305926321)
XLA Ops:
  0.6 0.0 copy-start
  0.6 0.0 copy-start.21
  0.7 0.0 copy-start.19
  0.7 0.0 copy-start.7
  0.7 1.1 %fusion = f32[24]{0:T(128)S(1)} fusion(bf16[24,2048]{1,0:T(8,128)(2,1)} %resid_ref.1), kind=kLoop, calls=%fused_computation.2 | loop fusion | flops 147432 | bytes 98400 | tf_op jit(solution)/shard_map/reduce_sum | solution.py:22
  1.8 0.1 constant_dynamic-slice_fusion.1
  1.9 0.8 constant_dynamic-slice_fusion
  2.7 0.1 fusion.3
  2.8 0.1 copy.40
  2.9 0.1 select_reduce_fusion
  3.0 0.1 copy.45
  3.0 0.7 convert_element_type.33
  3.7 0.7 reshape.57.gain_ref
  4.4 0.1 copy.43
  4.6 0.1 copy.41
  4.7 0.1 eq.40
  4.8 0.1 copy.42
  4.9 0.1 copy.46
  5.0 0.1 copy.44.select_ref
  5.1 1.0 fusion.2.normed_ref
  6.1 0.9 copy-done.8
  7.0 0.9 copy-done.9
  7.9 0.9 copy-done.10
  8.8 0.9 copy-done.11
  9.7 0.9 copy-done.12
  10.6 0.9 copy-done.13
  11.6 38.2 %shard_map.266.land_ref = bf16[32,24,192]{2,1,0:T(8,128)(2,1)S(1)} custom-call(bf16[24,2048]{1,0:T(8,128)(2,1)S(1)} %fusion.2.normed_ref, bf16[32,2048]{1,0:T(8,128)(2,1)S(1)} %bitcast.21, bf16[32,2048]{1,0:T(8,128)(2,1)S(1)} %bitcast.22, bf16[32,2048]{1,0:T(8,128)(2,1)S(1)} %bitcast.23, bf16[32,2048]{1,0:T(8,128)(2,1)S(1)} %bitcast.24, ...), custom_call_target="tpu_custom_call" | custom-call | flops 600000000 | bytes 100000000 | tf_op jit(solution)/shard_map/pallas_call | solution.py:321
  49.9 18.9 %shard_map.267 = (f32[24,16,4096]{2,1,0:T(8,128)}, f32[24,2048]{1,0:T(8,128)S(1)}, bf16[24,2048]{1,0:T(8,128)(2,1)S(1)}, bf16[32,4,2048]{2,1,0:T(4,128)(2,1)S(1)}) custom-call(bf16[32,24,192]{2,1,0:T(8,128)(2,1)S(1)} %shard_map.266.land_ref, bf16[2,192,768]{2,1,0:T(8,128)(2,1)S(1)} %copy-done.19, bf16[64,4096]{1,0:T(8,128)(2,1)S(1)} %copy-done.20, ...), custom_call_target="tpu_custom_call" | custom-call | flops 4000000000 | bytes 20000000 | tf_op jit(solution)/shard_map/pallas_call | solution.py:168
  68.9 1.6 %copy-done.5 = bf16[1,2048,512]{2,1,0:T(8,128)(2,1)S(1)} copy-done((bf16[1,2048,512]{2,1,0:T(8,128)(2,1)S(1)}, bf16[1,2048,512]{2,1,0:T(8,128)(2,1)}, u32[]{:S(2)}) %copy-start.5) | copy-done | bytes 2097176
  70.5 1.6 %copy-done.6 = bf16[1,512,2048]{2,1,0:T(8,128)(2,1)S(1)} copy-done((bf16[1,512,2048]{2,1,0:T(8,128)(2,1)S(1)}, bf16[1,512,2048]{2,1,0:T(8,128)(2,1)}, u32[]{:S(2)}) %copy-start.6) | copy-done | bytes 2097176
  72.1 34.8 %shard_map.268 = bf16[24,2048]{1,0:T(8,128)(2,1)S(1)} custom-call(bf16[32,4,2048]{2,1,0:T(4,128)(2,1)S(1)} %get-tuple-element.6.rows_ref, bf16[24,2048]{1,0:T(8,128)(2,1)S(1)} %get-tuple-element.7.normed_ref, f32[24,2048]{1,0:T(8,128)S(1)} %get-tuple-element.8.middle_ref, bf16[48,128]{1,0:T(8,128)(2,1)S(1)} %pad_maximum_fusion.coef_ref, ...), custom_call_target="tpu_custom_call" | custom-call | flops 1000000000 | bytes 60000000 | tf_op jit(solution)/shard_map/pallas_call | solution.py:435
  106.9 0.6 copy.48
  (44 shorter events, 0.3 us)
Async XLA Ops:
  0.6 1.2 %copy-start = (s32[768,4]{0,1:T(4,128)S(1)}, s32[768,4]{0,1:T(4,128)}, u32[]{:S(2)}) copy-start(s32[768,4]{0,1:T(4,128)} %param.42) | copy-start | bytes 36868
  0.6 49.1 %copy-start.21 = (bf16[256,256]{1,0:T(8,128)(2,1)S(1)}, bf16[256,256]{1,0:T(8,128)(2,1)}, u32[]{:S(2)}) copy-start(bf16[256,256]{1,0:T(8,128)(2,1)} %constant.33.clone.block_ref) | copy-start | bytes 393220
  0.7 49.1 %copy-start.19 = (bf16[2,192,768]{2,1,0:T(8,128)(2,1)S(1)}, bf16[2,192,768]{2,1,0:T(8,128)(2,1)}, u32[]{:S(2)}) copy-start(bf16[2,192,768]{2,1,0:T(8,128)(2,1)} %constant.30.clone.place_ref) | copy-start | bytes 1769476
  0.7 49.1 %copy-start.7 = (bf16[24,2048]{1,0:T(8,128)(2,1)S(1)}, bf16[24,2048]{1,0:T(8,128)(2,1)}, u32[]{:S(2)}) copy-start(bf16[24,2048]{1,0:T(8,128)(2,1)} %resid_ref.1) | copy-start | bytes 294916
  0.7 49.1 %copy-start.17 = (f32[1024]{0:T(1024)S(1)}, f32[1024]{0:T(1024)}, u32[]{:S(2)}) copy-start(f32[1024]{0:T(1024)} %param.38) | copy-start | bytes 12292
  0.7 49.1 %copy-start.16 = (f32[1024]{0:T(1024)S(1)}, f32[1024]{0:T(1024)}, u32[]{:S(2)}) copy-start(f32[1024]{0:T(1024)} %param.37) | copy-start | bytes 12292
  0.7 49.1 %copy-start.15 = (f32[1024]{0:T(1024)S(1)}, f32[1024]{0:T(1024)}, u32[]{:S(2)}) copy-start(f32[1024]{0:T(1024)} %param.36) | copy-start | bytes 12292
  0.7 49.1 %copy-start.14 = (f32[1024]{0:T(1024)S(1)}, f32[1024]{0:T(1024)}, u32[]{:S(2)}) copy-start(f32[1024]{0:T(1024)} %param.35) | copy-start | bytes 12292
  6.1 0.9 copy-start.8
  7.0 0.9 copy-start.9
  7.9 0.9 copy-start.10
  8.8 0.9 copy-start.11
  9.7 0.9 copy-start.12
  10.6 0.9 copy-start.13
  11.6 38.3 %copy-start.18 = (bf16[4096,128]{1,0:T(8,128)(2,1)S(1)}, bf16[4096,128]{1,0:T(8,128)(2,1)}, u32[]{:S(2)}) copy-start(bf16[4096,128]{1,0:T(8,128)(2,1)} %constant.32.clone.gather_ref) | copy-start | bytes 3145732
  11.6 38.3 %copy-start.20 = (bf16[64,4096]{1,0:T(8,128)(2,1)S(1)}, bf16[64,4096]{1,0:T(8,128)(2,1)}, u32[]{:S(2)}) copy-start(bf16[64,4096]{1,0:T(8,128)(2,1)} %constant.31.clone.spread_ref) | copy-start | bytes 1572868
  49.9 19.0 %copy-start.1 = (bf16[2048,512]{1,0:T(8,128)(2,1)S(1)}, bf16[2048,512]{1,0:T(8,128)(2,1)}, u32[]{:S(2)}) copy-start(bf16[2048,512]{1,0:T(8,128)(2,1)} %g0.1) | copy-start | bytes 6291460
  49.9 19.0 %copy-start.2 = (bf16[2048,512]{1,0:T(8,128)(2,1)S(1)}, bf16[2048,512]{1,0:T(8,128)(2,1)}, u32[]{:S(2)}) copy-start(bf16[2048,512]{1,0:T(8,128)(2,1)} %g1.1) | copy-start | bytes 6291460
  49.9 19.0 %copy-start.3 = (bf16[512,2048]{1,0:T(8,128)(2,1)S(1)}, bf16[512,2048]{1,0:T(8,128)(2,1)}, u32[]{:S(2)}) copy-start(bf16[512,2048]{1,0:T(8,128)(2,1)} %g2.1) | copy-start | bytes 6291460
  49.9 19.0 %copy-start.4 = (bf16[1,2048,512]{2,1,0:T(8,128)(2,1)S(1)}, bf16[1,2048,512]{2,1,0:T(8,128)(2,1)}, u32[]{:S(2)}) copy-start(bf16[1,2048,512]{2,1,0:T(8,128)(2,1)} %param.44) | copy-start | bytes 6291460
  68.9 1.6 %copy-start.5 = (bf16[1,2048,512]{2,1,0:T(8,128)(2,1)S(1)}, bf16[1,2048,512]{2,1,0:T(8,128)(2,1)}, u32[]{:S(2)}) copy-start(bf16[1,2048,512]{2,1,0:T(8,128)(2,1)} %param.45) | copy-start | bytes 6291460
  70.5 1.6 %copy-start.6 = (bf16[1,512,2048]{2,1,0:T(8,128)(2,1)S(1)}, bf16[1,512,2048]{2,1,0:T(8,128)(2,1)}, u32[]{:S(2)}) copy-start(bf16[1,512,2048]{2,1,0:T(8,128)(2,1)} %param.46) | copy-start | bytes 6291460
where the time goes:
time: 108 us
  Pallas kernels  91.9 us (85%)
  local copies, waits for them, and re-layouts  11.6 us (11%)
  other arithmetic  3.06 us (3%)
    pallas_call x1, Pallas kernels, project(): pl.pallas_call(functools.partial(project_kernel, depth), out_shape=jax.Sh...  38.2 us
    pallas_call x1, Pallas kernels, experts_step(): pl.pallas_call(functools.partial(experts_kernel, depth), out_shape=jax.Sh...  34.8 us
    pallas_call x1, Pallas kernels, mixer(): pl.pallas_call(mixer_kernel, grid=(tokens // group,), out_shape=(jax.Shap...  18.9 us
    unnamed x45, local copies, waits for them, and re-layouts  9.32 us

commit v1 on v0

v1 whole, which is shorter than its diff:
```python
import functools
import math

import jax
import jax.numpy as jnp
from jax import lax
from jax.experimental import pallas as pl
from jax.experimental.pallas import tpu as pltpu
from jax.sharding import PartitionSpec as P

HEAD_COUNT = 16
HEAD_SIZE = 64
CAP = 4
ROLES = 6
LANES = 128
F32 = jnp.float32
BF16 = jnp.bfloat16


def rms_norm(value_rows, gain):
    scale = lax.rsqrt(jnp.mean(value_rows * value_rows, axis=-1, keepdims=True) + 1e-06)
    return (value_rows * scale * gain.astype(F32)).astype(BF16)


def expert_mlp(rows, gate_w, up_w, down_w):
    gate = jnp.dot(rows, gate_w, preferred_element_type=F32)
    upward = jnp.dot(rows, up_w, preferred_element_type=F32)
    hidden = (jax.nn.silu(gate) * upward).astype(BF16)
    return jnp.dot(hidden, down_w, preferred_element_type=F32).astype(BF16)


def split(value):
    high = value.astype(BF16)
    return high, (value - high.astype(F32)).astype(BF16)


def dot(a, b):
    return jnp.dot(a, b, preferred_element_type=F32)


PLANE = 8
CORES = 2
COLUMNS = PLANE // CORES


def remote(source, target, device, send_sem, recv_sem):
    return pltpu.make_async_remote_copy(
        src_ref=source, dst_ref=target, send_sem=send_sem, recv_sem=recv_sem,
        device_id={"ep": device}, device_id_type=pl.DeviceIdType.MESH,
    )


def route_tables(routes, weights, me, tokens, select_out, coef_out):
    everyone = routes.shape[1]
    slots = select_out.shape[1]
    contract = (((1,), (1,)), ((), ()))
    mine = lax.broadcasted_iota(jnp.int32, (tokens, everyone), 1) - me * tokens
    pick = (mine == lax.broadcasted_iota(jnp.int32, (tokens, everyone), 0)).astype(F32).astype(BF16)

    def own(table):
        return lax.dot_general(pick, table, contract, preferred_element_type=F32)

    named = own(routes.astype(F32).astype(BF16))
    weight_high, weight_low = split(weights)
    own_high, own_low = own(weight_high), own(weight_low)
    lane = lax.broadcasted_iota(jnp.int32, (tokens, slots), 1)
    expert = (lane // CAP).astype(F32)
    hit = jnp.zeros((tokens, slots), F32)
    high, low = hit, hit
    for entry in range(routes.shape[0]):
        match = (named[:, entry : entry + 1] == expert).astype(F32)
        hit = hit + match
        high = high + match * own_high[:, entry : entry + 1]
        low = low + match * own_low[:, entry : entry + 1]
    later = lax.broadcasted_iota(jnp.int32, (tokens, tokens), 0)
    earlier = lax.broadcasted_iota(jnp.int32, (tokens, tokens), 1)
    before = (earlier < later).astype(F32).astype(BF16)
    rank = dot(before, hit.astype(BF16))
    chosen = hit * (rank == (lane % CAP).astype(F32)).astype(F32)
    select_out[...] = chosen
    coef_out[:tokens] = (chosen * high).astype(BF16)
    coef_out[tokens:] = (chosen * low).astype(BF16)


def place_matrix(piece, rows, width):
    lane = lax.broadcasted_iota(jnp.int32, (1, ROLES * LANES), 1)
    inner = lane % HEAD_SIZE - piece * CORES * width
    core = inner // width
    row = (core * ROLES + lane // LANES) * width + inner - core * width
    row = jnp.where((inner >= 0) & (inner < CORES * width), row, -1)
    here = lax.broadcasted_iota(jnp.int32, (rows, ROLES * LANES), 0)
    return (here == row).astype(F32).astype(BF16)


def gather_matrix(first, columns):
    value = first + lax.broadcasted_iota(jnp.int32, (columns, LANES), 0) // HEAD_SIZE
    lane = lax.broadcasted_iota(jnp.int32, (columns, LANES), 1) % HEAD_SIZE
    return (value == lane).astype(F32).astype(BF16)


def spread_matrix(first, columns):
    value = first + lax.broadcasted_iota(jnp.int32, (LANES, columns), 1) // HEAD_SIZE
    row = lax.broadcasted_iota(jnp.int32, (LANES, columns), 0) % HEAD_SIZE
    return (value == row).astype(F32).astype(BF16)


def gain_row(gain):
    rows = gain.astype(F32)
    return jnp.concatenate([rows[i : i + 1] for i in range(rows.shape[0])], axis=1)


PARTS = 4


def layer_kernel(
    depth,
    resid_hbm, gain_hbm, w0, w1, w2, w3, w4, w5, routes_hbm, rweight_hbm,
    const0, const1, const2, const3, state_hbm, out_w_hbm, ffn_gain_hbm, g0, g1, g2, g3, g4, g5,
    hidden_out, recalled_out, value_out, decay_out, removal_out, scaled_out,
    resid, gain, weight, routes, rweight, held, cols, land,
    raw, consts, state, out_w, ffn_gain, b0, b1, b2, b3, b4, b5,
    place, role_ref, unit_ref, query_ref, mixed_ref, select_ref, coef_ref,
    middle_ref, normed_ref, out_rows, served, output, returned,
    load_sem, weight_sem, state_sem, big_sem,
    z_send, z_recv, near_send, near_recv, half_send, half_recv, mate_send, mate_recv,
    out_send, out_recv, go_send, go_recv, back_send, back_recv,
):
    total = depth * PLANE
    chips = depth * COLUMNS
    tokens, model = resid_hbm.shape
    cut = model // 2
    me = lax.axis_index("ep")
    core = lax.rem(me, CORES)
    chip = me // CORES
    column = lax.rem(chip, COLUMNS)
    level = chip // COLUMNS
    x = lax.rem(column, 2)
    y = column // 2
    mate = me + 1 - 2 * core
    column_x = column + 1 - 2 * x
    column_y = column + 2 - 4 * y
    far = COLUMNS - 1 - column
    pieces = land.shape[1]
    rows_all = tokens * HEAD_COUNT

    def device(of_level, of_column):
        return (of_level * COLUMNS + of_column) * CORES + core

    along_x, along_y = device(level, column_x), device(level, column_y)

    barrier = pltpu.get_barrier_semaphore()

    def greet(number, carry):
        peer = lax.rem(me + number, total)
        pl.semaphore_signal(barrier, inc=1, device_id={"ep": peer}, device_id_type=pl.DeviceIdType.MESH)
        return carry

    lax.fori_loop(1, total, greet, 0)

    loads = [
        pltpu.make_async_copy(source, target, load_sem.at[i])
        for i, (source, target) in enumerate(
            (
                (resid_hbm, resid), (gain_hbm, gain), (routes_hbm, routes), (rweight_hbm, rweight),
                (const0, raw.at[0]), (const1, raw.at[1]), (const2, raw.at[2]), (const3, raw.at[3]),
                (ffn_gain_hbm, ffn_gain),
            )
        )
    ]
    for load in loads:
        load.start()
    weight_loads = [
        pltpu.make_async_copy(source, weight.at[core, i], weight_sem.at[i])
        for i, source in enumerate((w0, w1, w2, w3, w4, w5))
    ]
    for load in weight_loads:
        load.start()
    span = state.shape[2] // PARTS
    state_loads = [
        pltpu.make_async_copy(
            state_hbm.at[:, :, pl.ds(i * span, span)], state.at[:, :, pl.ds(i * span, span)], state_sem.at[i]
        )
        for i in range(PARTS)
    ]
    big_loads = [
        pltpu.make_async_copy(source, target, big_sem.at[i])
        for i, (source, target) in enumerate(
            ((out_w_hbm, out_w), (g0, b0), (g1, b1), (g2, b2), (g3, b3), (g4, b4), (g5, b5))
        )
    ]

    loads[0].wait()
    loads[1].wait()
    held[column, level] = rms_norm(resid[...].astype(F32), gain_row(gain[...]))
    for load in weight_loads:
        load.wait()
    for load in state_loads + big_loads:
        load.start()

    pl.semaphore_wait(barrier, total - 1)

    nearer = jnp.minimum(level, depth - 1 - level)

    def nearest(k):
        step = (k + 1) // 2 if k % 2 else -(k // 2)
        beyond = jnp.where(2 * level < depth - 1, k - nearer, nearer - k)
        return level + jnp.where(k <= 2 * nearer, step, beyond)

    order = [level] + [nearest(k) for k in range(1, depth)]

    def along_z(to, source, slot):
        return remote(held.at[column, slot], held.at[column, slot], device(to, column), z_send.at[to], z_recv.at[source])

    for to in order[1:]:
        along_z(to, level, level).start()

    sent = []

    def forward(slot):
        block = held.at[column, slot]
        for axis, target in ((0, along_y), (1, along_x)):
            copy = remote(block, block, target, near_send.at[axis, slot], near_recv.at[axis, slot])
            copy.start()
            sent.append(copy)

    def relay(slot):
        for axis, (of_column, target, part) in enumerate(
            ((column_y, along_x, slice(0, cut)), (column_x, along_y, slice(cut, model)))
        ):
            block = held.at[of_column, slot]
            remote(block, block, along_y, near_send.at[axis, slot], near_recv.at[axis, slot]).wait_recv()
            half = block.at[:, part]
            copy = remote(half, half, target, half_send.at[axis, slot], half_recv.at[axis, slot])
            copy.start()
            sent.append(copy)

    forward(level)
    swap = remote(weight.at[core], weight.at[core], mate, mate_send, mate_recv)
    swap.start()
    for load in loads[2:]:
        load.wait()
    route_tables(routes[...], rweight[...], me, tokens, select_ref, coef_ref)
    for number in range(4):
        pair = raw[number]
        turned = pltpu.roll(pair, HEAD_SIZE, 1)
        first = lax.broadcasted_iota(jnp.int32, pair.shape, 1) < HEAD_SIZE
        count = pair.shape[0]
        consts[number, pl.ds(0, count, stride=2), :] = jnp.where(first, pair, turned)
        consts[number, pl.ds(1, count, stride=2), :] = jnp.where(first, turned, pair)
    for piece in range(pieces):
        place[piece] = place_matrix(piece, place.shape[1], weight.shape[2])

    for before, slot in zip(order, order[1:]):
        along_z(slot, slot, slot).wait_recv()
        forward(slot)
        relay(before)
    swap.wait_recv()

    def compute(of_column):
        rows = held[of_column].astype(F32).reshape(depth * tokens, model).astype(BF16)
        both = weight[...]
        width = both.shape[2]
        if width % 16:
            both = both.astype(F32)
        both = both.reshape(CORES * ROLES * width, model).astype(BF16)
        result = lax.dot_general(rows, both, (((1,), (1,)), ((), ())), preferred_element_type=F32)
        cols[of_column] = result.reshape(depth, tokens, result.shape[-1]).astype(BF16)

    def handed(of_level, of_column):
        to_chip = of_level * COLUMNS + of_column
        number = lax.rem(to_chip - chip + chips, chips)
        return remote(
            cols.at[of_column, of_level], land.at[chip // pieces, lax.rem(chip, pieces)], to_chip * CORES + core,
            out_send.at[number], out_recv.at[number],
        )

    def give(of_column):
        for to in order:
            if of_column is column and to is level:
                land[chip // pieces, lax.rem(chip, pieces)] = cols[column, level]
            else:
                handed(to, of_column).start()

    compute(column)
    relay(order[-1])
    give(column)
    compute(column_y)
    give(column_y)
    compute(column_x)
    give(column_x)
    for slot in order:
        for axis, part in ((0, slice(0, cut)), (1, slice(cut, model))):
            half = held.at[far, slot].at[:, part]
            remote(half, half, along_x, half_send.at[axis, slot], half_recv.at[axis, slot]).wait_recv()
    compute(far)
    give(far)

    def finish(number, carry):
        to_chip = lax.rem(chip + number, chips)
        copy = remote(
            cols.at[0, 0], land.at[0, 0], to_chip * CORES + core, out_send.at[number], out_recv.at[number]
        )
        copy.wait_recv()
        copy.wait_send()
        return carry

    lax.fori_loop(1, chips, finish, 0)

    spread_out = jnp.zeros((rows_all, ROLES * LANES), F32)
    for piece in range(pieces):
        rows = land[:, piece].astype(F32).reshape(rows_all, land.shape[3]).astype(BF16)
        spread_out = spread_out + dot(rows, place[piece])
    for head in range(HEAD_COUNT):
        for number in range(ROLES):
            part = spread_out[head * tokens : (head + 1) * tokens, number * LANES : (number + 1) * LANES]
            role_ref[number, pl.ds(head, tokens, stride=HEAD_COUNT), :] = part

    def const(number):
        one = consts[number]
        return jnp.concatenate([one] * tokens, axis=0)

    half_lanes = HEAD_SIZE / LANES

    def head_sum(value):
        return jnp.sum(value, axis=-1, keepdims=True) * half_lanes

    receptance, keys, values = role_ref[0], role_ref[1], role_ref[2]
    decay = jnp.exp(-math.exp(-0.5) * jax.nn.sigmoid(const(0) + role_ref[3]))
    rate = jax.nn.sigmoid(const(1) + role_ref[4])
    unit_key = keys * lax.rsqrt(1.0 + head_sum(keys * keys))
    scaled_key = keys * rate
    removal = unit_key * rate
    self_sum = head_sum(receptance * scaled_key * const(2))
    removed = head_sum(removal * receptance)
    added = head_sum(scaled_key * receptance)
    unit_ref[...] = unit_key
    query_ref[...] = decay * receptance
    value_out[...] = values
    decay_out[...] = decay
    removal_out[...] = removal
    scaled_out[...] = scaled_key

    recalled = jnp.zeros((rows_all, LANES), F32)
    kept = jnp.zeros((rows_all, LANES), F32)
    for part in range(PARTS):
        state_loads[part].wait()
        pick = gather_matrix(part * span // HEAD_SIZE, span)
        block = state[:, :, part * span : (part + 1) * span].reshape(rows_all, span)
        wide_key = jnp.concatenate([unit_ref[...]] * (span // LANES), axis=1)
        recalled = recalled + dot((block * wide_key).astype(BF16), pick)
        wide_query = jnp.concatenate([query_ref[...]] * (span // LANES), axis=1)
        kept = kept + dot((block * wide_query).astype(BF16), pick)
    recalled_out[...] = recalled
    values = role_ref[2]
    read = kept - recalled * removed + values * added
    centered = read - head_sum(read) * (1.0 / HEAD_SIZE)
    variance = head_sum(centered * centered) * (1.0 / HEAD_SIZE)
    normal = centered * lax.rsqrt(variance + 0.00064) * const(3)
    mixed_ref[...] = (normal + self_sum * values) * jax.nn.sigmoid(role_ref[5])

    lane = lax.broadcasted_iota(jnp.int32, (tokens, LANES), 1)
    per = LANES // HEAD_SIZE
    parts = []
    for first in range(0, HEAD_COUNT, per):
        part = mixed_ref[pl.ds(first, tokens, stride=HEAD_COUNT), :]
        for other in range(1, per):
            rest = mixed_ref[pl.ds(first + other, tokens, stride=HEAD_COUNT), :]
            part = jnp.where(lane < other * HEAD_SIZE, part, rest)
        parts.append(part.astype(BF16))
    mixed = jnp.concatenate(parts, axis=1)
    big_loads[0].wait()
    attended = dot(mixed, out_w[...]).astype(BF16).astype(F32)
    middle = resid[...].astype(F32) + attended
    middle_ref[...] = middle
    normed = rms_norm(middle, gain_row(ffn_gain[...]))
    normed_ref[...] = normed
    picked = lax.dot_general(
        select_ref[...].astype(BF16), normed, (((0,), (0,)), ((), ())), preferred_element_type=F32
    )
    out_rows[...] = picked.reshape(out_rows.shape).astype(BF16)

    def go(number):
        to = lax.rem(me + number, total)
        return remote(out_rows.at[to], served.at[me], to, go_send.at[number], go_recv.at[number])

    def back(to):
        number = lax.rem(to - me + total, total)
        return remote(output.at[to], returned.at[me], to, back_send.at[number], back_recv.at[number])

    def launch(number, carry):
        go(number).start()
        return carry

    lax.fori_loop(1, total, launch, 0)
    served[me] = out_rows[me]
    for load in big_loads[1:4]:
        load.wait()
    shared = expert_mlp(normed_ref[...], b0[...], b1[...], b2[...])
    middle_ref[...] = middle_ref[...] + shared.astype(F32)
    for load in big_loads[4:]:
        load.wait()

    for d in range(depth):
        first = lax.rem(level + depth - d, depth) * PLANE

        def arrive(i, carry):
            source = first + i

            @pl.when(source != me)
            def _():
                go(lax.rem(me - source + total, total)).wait_recv()

            return carry

        lax.fori_loop(0, PLANE, arrive, 0)
        rows = served[pl.ds(first, PLANE)].reshape(PLANE * CAP, model)
        result = expert_mlp(rows, b3[...], b4[...], b5[...])
        output[pl.ds(first, PLANE)] = result.reshape(PLANE, CAP, model)

        def give_back(i, carry):
            source = first + i

            @pl.when(source != me)
            def _():
                back(source).start()

            return carry

        lax.fori_loop(0, PLANE, give_back, 0)
    returned[me] = output[me]

    def ended(number, carry):
        go(number).wait_send()
        copy = back(lax.rem(me + number, total))
        copy.wait_recv()
        copy.wait_send()
        return carry

    lax.fori_loop(1, total, ended, 0)
    routed = dot(coef_ref[...], returned[...].reshape(total * CAP, model))
    hidden_out[...] = (middle_ref[...] + (routed[:tokens] + routed[tokens:])).astype(BF16)

    for to in order[1:]:
        along_z(to, level, level).wait_send()
    for copy in sent:
        copy.wait_send()
    swap.wait_send()


def layer(resid, gain, weights, routes, routing_weight, consts, state, out_w, ffn_gain, experts, ep_size):
    depth = ep_size // PLANE
    chips = ep_size // CORES
    pieces = chips // HEAD_COUNT
    tokens, model = resid.shape
    weights = [w.T for w in weights]
    width = weights[0].shape[0]
    wide = CORES * ROLES * width
    rows_all = tokens * HEAD_COUNT
    routes, routing_weight = routes.T, routing_weight.T
    gain = gain.reshape(model // LANES, LANES)
    ffn_gain = ffn_gain.reshape(model // LANES, LANES)
    consts = [c.reshape(-1, LANES) for c in consts]
    slots = ep_size * CAP
    dma = pltpu.SemaphoreType.DMA
    hbm = pl.BlockSpec(memory_space=pltpu.HBM)
    vmem = pl.BlockSpec(memory_space=pltpu.VMEM)
    operands = (resid, gain, *weights, routes, routing_weight, *consts, state, out_w, ffn_gain, *experts)
    operands = [pltpu.with_memory_space_constraint(a, pltpu.HBM) for a in operands]
    lanes = jax.ShapeDtypeStruct((rows_all, LANES), F32)
    return pl.pallas_call(
        functools.partial(layer_kernel, depth),
        out_shape=(jax.ShapeDtypeStruct((tokens, model), BF16),) + (lanes,) * 5,
        in_specs=[hbm] * len(operands),
        out_specs=(vmem,) * 6,
        scratch_shapes=[
            pltpu.VMEM((tokens, model), BF16),
            pltpu.VMEM(gain.shape, BF16),
            pltpu.VMEM((CORES, ROLES, width, model), BF16),
            pltpu.VMEM(routes.shape, jnp.int32),
            pltpu.VMEM(routes.shape, F32),
            pltpu.VMEM((COLUMNS, depth, tokens, model), BF16),
            pltpu.VMEM((COLUMNS, depth, tokens, wide), BF16),
            pltpu.VMEM((HEAD_COUNT, pieces, tokens, wide), BF16),
            pltpu.VMEM((4,) + consts[0].shape, F32),
            pltpu.VMEM((4, HEAD_COUNT, LANES), F32),
            pltpu.VMEM(state.shape, F32),
            pltpu.VMEM(out_w.shape, BF16),
            pltpu.VMEM(gain.shape, BF16),
        ]
        + [pltpu.VMEM(w.shape, BF16) for w in experts]
        + [
            pltpu.VMEM((pieces, wide, ROLES * LANES), BF16),
            pltpu.VMEM((ROLES, rows_all, LANES), F32),
            pltpu.VMEM((rows_all, LANES), F32),
            pltpu.VMEM((rows_all, LANES), F32),
            pltpu.VMEM((rows_all, LANES), F32),
            pltpu.VMEM((tokens, slots), F32),
            pltpu.VMEM((2 * tokens, slots), BF16),
            pltpu.VMEM((tokens, model), F32),
            pltpu.VMEM((tokens, model), BF16),
        ]
        + [pltpu.VMEM((ep_size, CAP, model), BF16)] * 4
        + [
            dma((9,)), dma((ROLES,)), dma((PARTS,)), dma((7,)),
            dma((depth,)), dma((depth,)),
            dma((2, depth)), dma((2, depth)),
            dma((2, depth)), dma((2, depth)),
            dma, dma,
            dma((chips,)), dma((chips,)),
        ]
        + [dma((ep_size,))] * 4,
        compiler_params=pltpu.CompilerParams(
            has_side_effects=True, collective_id=0, vmem_limit_bytes=52 * 1024 * 1024
        ),
        cost_estimate=pl.CostEstimate(flops=30_000_000_000, bytes_accessed=100_000_000, transcendentals=0),
    )(*operands)


def update_kernel(
    state, recalled, value, decay, removal, scaled, hidden, next_hbm, hidden_hbm, held, next_sem, hidden_sem
):
    copy = pltpu.make_async_copy(hidden, hidden_hbm, hidden_sem)
    copy.start()
    group, heads, columns = state.shape
    rows_all = group * heads
    span = columns // PARTS
    step = 4 * HEAD_SIZE
    lane = lax.broadcasted_iota(jnp.int32, (rows_all, LANES), 1)
    high, low = split(recalled[...])
    both = jnp.where(lane < HEAD_SIZE, high.astype(F32), low.astype(F32)).astype(BF16)
    alone = jnp.where(lane < HEAD_SIZE, value[...], 0.0).astype(BF16)
    stacked = jnp.concatenate([both, alone], axis=0)

    def twice(ref):
        return jnp.concatenate([ref[...]] * (step // LANES), axis=1)

    copies = []
    for part in range(PARTS):
        for first in range(part * span, (part + 1) * span, step):
            spread = dot(stacked, spread_matrix(first // HEAD_SIZE, step))
            block = state[:, :, first : first + step].reshape(rows_all, step)
            new = block * twice(decay) - spread[:rows_all] * twice(removal) + spread[rows_all:] * twice(scaled)
            held[:, :, first : first + step] = new.reshape(group, heads, step)
        here = pl.ds(part * span, span)
        out = pltpu.make_async_copy(held.at[:, :, here], next_hbm.at[:, :, here], next_sem.at[part])
        out.start()
        copies.append(out)
    for out in copies:
        out.wait()
    copy.wait()


def update(state, recalled, value, decay, removal, scaled, hidden):
    vmem = pl.BlockSpec(memory_space=pltpu.VMEM)
    hbm = pl.BlockSpec(memory_space=pltpu.HBM)
    dma = pltpu.SemaphoreType.DMA
    return pl.pallas_call(
        update_kernel,
        out_shape=(
            jax.ShapeDtypeStruct(state.shape, F32),
            jax.ShapeDtypeStruct(hidden.shape, BF16),
        ),
        in_specs=[vmem] * 7,
        out_specs=(hbm, hbm),
        scratch_shapes=[pltpu.VMEM(state.shape, F32), dma((PARTS,)), dma],
        compiler_params=pltpu.CompilerParams(vmem_limit_bytes=20 * 1024 * 1024),
        cost_estimate=pl.CostEstimate(flops=1_000_000_000, bytes_accessed=20_000_000, transcendentals=0),
    )(state, recalled, value, decay, removal, scaled, hidden)


def per_device(
    residual_input,
    attention_norm_gain,
    receptance_weight,
    key_weight,
    value_weight,
    decay_weight,
    correction_rate_weight,
    output_gate_weight,
    decay_offset,
    correction_rate_offset,
    self_term_weight,
    head_read_gain,
    previous_state,
    attention_output_weight,
    feedforward_norm_gain,
    routes,
    routing_weight,
    routed_gate_weight,
    routed_up_weight,
    routed_down_weight,
    common_gate_weight,
    common_up_weight,
    common_down_weight,
):
    ep_size = lax.axis_size("ep")
    hidden, recalled, value, decay, removal, scaled = layer(
        residual_input,
        attention_norm_gain,
        (
            receptance_weight,
            key_weight,
            value_weight,
            decay_weight,
            correction_rate_weight,
            output_gate_weight,
        ),
        routes,
        routing_weight,
        (decay_offset, correction_rate_offset, self_term_weight, head_read_gain),
        previous_state,
        attention_output_weight,
        feedforward_norm_gain,
        (
            common_gate_weight,
            common_up_weight,
            common_down_weight,
            routed_gate_weight[0],
            routed_up_weight[0],
            routed_down_weight[0],
        ),
        ep_size,
    )
    next_state, hidden_out = update(previous_state, recalled, value, decay, removal, scaled, hidden)
    return (hidden_out, next_state)


def solution(mesh):
    return jax.shard_map(
        per_device,
        mesh=mesh,
        in_specs=(
            P(("grp", "ep"), None),
            P(),
            P(None, "ep"),
            P(None, "ep"),
            P(None, "ep"),
            P(None, "ep"),
            P(None, "ep"),
            P(None, "ep"),
            P(),
            P(),
            P(),
            P(),
            P(("grp", "ep"), None, None),
            P(),
            P(),
            P("grp", None),
            P("grp", None),
            P("ep", None, None),
            P("ep", None, None),
            P("ep", None, None),
            P(),
            P(),
            P(),
        ),
        out_specs=(P(("grp", "ep"), None), P(("grp", "ep"), None, None)),
        check_vma=False,
    )
```

time: 108 us -> 67.9 us (0.63)
  Pallas kernels: 91.9 us -> 67.1 us
  local copies, waits for them, and re-layouts: 11.6 us -> 0.01 us
  other arithmetic: 3.06 us -> 0.01 us
    pallas_call x3 -> x2, Pallas kernels: 91.9 us -> 67.1 us  [the longest x1 63.7 us: layer(): pl.pallas_call(functools.partial(layer_kernel, depth), out_shape=(jax.Sha...]
    unnamed x45 -> x4, local copies, waits for them, and re-layouts: 9.32 us -> 0.01 us
    convert_element_type x5 -> x0, other arithmetic: 1.73 us -> none  [the longest x2 1.68 us: rms_norm(): return (value_rows * scale * gain.astype(F32)).astype(BF16)]
    reduce_sum x2 -> x0, other arithmetic: 1.18 us -> none  [the longest x1 1.09 us: rms_norm(): jnp.mean(value_rows * value_rows, axis=-1, keepdims=True) + 1e-06]
where the time goes in v1:
time: 67.9 us; the launch traced here: 67.8 us
  Pallas kernels  67.1 us (99%)
  between operations  0.69 us (1%)
    pallas_call x1, Pallas kernels, layer(): pl.pallas_call(functools.partial(layer_kernel, depth), out_shape=(jax.Sha...  63.7 us
    pallas_call x1, Pallas kernels, update(): pl.pallas_call(update_kernel, out_shape=(jax.ShapeDtypeStruct(state.shape...  3.41 us

profile of v1, /device:TPU:0, one launch (start us, length us, event | category | flops | bytes accessed | tf_op | source)
XLA Modules:
  0.0 67.8 jit_solution(18179730704033870045)
XLA Ops:
  0.6 0.0 slice-start
  0.6 0.0 slice-start.1
  0.7 63.7 %shard_map.230 = (bf16[24,2048]{1,0:T(8,128)(2,1)S(1)}, f32[384,128]{1,0:T(8,128)S(1)}, f32[384,128]{1,0:T(8,128)S(1)}, f32[384,128]{1,0:T(8,128)S(1)}, f32[384,128]{1,0:T(8,128)S(1)}, /*index=5*/f32[384,128]{1,0:T(8,128)S(1)}) custom-call(bf16[24,2048]{1,0:T(8,128)(2,1)} %resid_hbm.1, bf16[16,128]{1,0:T(8,128)(2,1)} %bitcast.30, bf16[32,2048]{1,0:T(8,128)(2,1)} %bitcast.22, ...), custom_call_target="tpu_custom_call" | custom-call | flops 30000001024 | bytes 100000000 | tf_op jit(solution)/shard_map/pallas_call | solution.py:470
  64.3 0.0 slice-done
  64.3 0.0 slice-done.1
  64.4 3.4 %shard_map.231 = (f32[24,16,4096]{2,1,0:T(8,128)}, bf16[24,2048]{1,0:T(8,128)(2,1)}) custom-call(f32[24,16,4096]{2,1,0:T(8,128)S(1)} %bitcast.18, f32[384,128]{1,0:T(8,128)S(1)} %get-tuple-element.10.recalled, f32[384,128]{1,0:T(8,128)S(1)} %get-tuple-element.11.value, f32[384,128]{1,0:T(8,128)S(1)} %get-tuple-element.12.decay, ...), custom_call_target="tpu_custom_call" | custom-call | flops 1000000000 | bytes 20000000 | tf_op jit(solution)/shard_map/pallas_call | solution.py:557
  (1 shorter events, 0.0 us)
Async XLA Ops:
  0.6 63.7 %slice-start = ((s8[6291456]{0:T(1024)(128)(4,1)}), s8[4194304]{0:T(1024)(128)(4,1)S(1)}, s32[]{:S(2)}) async-start(s8[6291456]{0:T(1024)(128)(4,1)} %bitcast.17), calls=%async_computation | async-start | bytes 8388608
  0.6 63.7 %slice-start.1 = ((s8[6291456]{0:T(1024)(128)(4,1)}), s8[2097152]{0:T(1024)(128)(4,1)S(1)}, s32[]{:S(2)}) async-start(s8[6291456]{0:T(1024)(128)(4,1)} %bitcast.17), calls=%async_computation.1 | async-start | bytes 4194304

commit v2 on v1

--- a/solution.py
+++ b/solution.py
@@ -110,16 +110,18 @@
 
 
 PARTS = 4
+STORES = 8
+UNITS = 2
 
 
 def layer_kernel(
     depth,
     resid_hbm, gain_hbm, w0, w1, w2, w3, w4, w5, routes_hbm, rweight_hbm,
     const0, const1, const2, const3, state_hbm, out_w_hbm, ffn_gain_hbm, g0, g1, g2, g3, g4, g5,
-    hidden_out, recalled_out, value_out, decay_out, removal_out, scaled_out,
+    hidden_out, state,
     resid, gain, weight, routes, rweight, held, cols, land,
-    raw, consts, state, out_w, ffn_gain, b0, b1, b2, b3, b4, b5,
-    place, role_ref, unit_ref, query_ref, mixed_ref, select_ref, coef_ref,
+    raw, consts, out_w, ffn_gain, b0, b1, b2, b3, b4, b5,
+    place, role_ref, unit_ref, query_ref, mixed_ref, recalled_ref, decay_ref, removal_ref, scaled_ref, select_ref, coef_ref,
     middle_ref, normed_ref, out_rows, served, output, returned,
     load_sem, weight_sem, state_sem, big_sem,
     z_send, z_recv, near_send, near_recv, half_send, half_recv, mate_send, mate_recv,
@@ -128,7 +130,7 @@
     total = depth * PLANE
     chips = depth * COLUMNS
     tokens, model = resid_hbm.shape
-    cut = model // 2
+    cut = model // UNITS
     me = lax.axis_index("ep")
     core = lax.rem(me, CORES)
     chip = me // CORES
@@ -150,13 +152,6 @@
 
     barrier = pltpu.get_barrier_semaphore()
 
-    def greet(number, carry):
-        peer = lax.rem(me + number, total)
-        pl.semaphore_signal(barrier, inc=1, device_id={"ep": peer}, device_id_type=pl.DeviceIdType.MESH)
-        return carry
-
-    lax.fori_loop(1, total, greet, 0)
-
     loads = [
         pltpu.make_async_copy(source, target, load_sem.at[i])
         for i, (source, target) in enumerate(
@@ -167,7 +162,17 @@
             )
         )
     ]
-    for load in loads:
+    for load in loads[:2]:
+        load.start()
+
+    def greet(number, carry):
+        peer = lax.rem(me + number, total)
+        pl.semaphore_signal(barrier, inc=1, device_id={"ep": peer}, device_id_type=pl.DeviceIdType.MESH)
+        return carry
+
+    lax.fori_loop(1, total, greet, 0)
+
+    for load in loads[2:]:
         load.start()
     weight_loads = [
         pltpu.make_async_copy(source, weight.at[core, i], weight_sem.at[i])
@@ -192,49 +197,70 @@
     loads[0].wait()
     loads[1].wait()
     held[column, level] = rms_norm(resid[...].astype(F32), gain_row(gain[...]))
+    pl.semaphore_wait(barrier, total - 1)
+
+    nearer = jnp.minimum(level, depth - 1 - level)
+
+    def nearest(k):
+        step = (k + 1) // 2 if k % 2 else -(k // 2)
+        beyond = jnp.where(2 * level < depth - 1, k - nearer, nearer - k)
+        return level + jnp.where(k <= 2 * nearer, step, beyond)
+
+    order = [level] + [nearest(k) for k in range(1, depth)]
+
+    halves = [slice(i * cut, (i + 1) * cut) for i in range(UNITS)]
+    turns = UNITS // 2
+
+    def along_z(to, slot, half):
+        block = held.at[column, slot].at[:, halves[half]]
+        downward = jnp.where(to > level, 0, 1)
+        return remote(
+            block, block, device(to, column), z_send.at[downward, slot, half], z_recv.at[slot, half]
+        )
+
+    def each_way(act):
+        for half in range(UNITS):
+            for to in (level + 1, level - 1):
+
+                @pl.when((to >= 0) & (to < depth))
+                def _():
+                    act(along_z(to, level, half))
+
+    def onward(slot, half, act):
+        to = jnp.where(slot > level, level - 1, level + 1)
+
+        @pl.when((to >= 0) & (to < depth))
+        def _():
+            act(along_z(to, slot, half))
+
+    each_way(lambda copy: copy.start())
+    sent = []
+
+    def near(axis, of_column, slot, half, target):
+        block = held.at[of_column, slot].at[:, halves[half]]
+        return remote(block, block, target, near_send.at[axis, slot, half], near_recv.at[axis, slot, half])
+
+    def forward(slot, half):
+        for axis, target in ((0, along_y), (1, along_x)):
+            copy = near(axis, column, slot, half, target)
+            copy.start()
+            sent.append(copy)
+
+    def relay(slot, turn):
+        for axis, (of_column, target) in enumerate(((column_y, along_x), (column_x, along_y))):
+            unit = axis * turns + turn
+            near(axis, of_column, slot, unit, target).wait_recv()
+            block = held.at[of_column, slot].at[:, halves[unit]]
+            copy = remote(block, block, target, half_send.at[slot, unit], half_recv.at[slot, unit])
+            copy.start()
+            sent.append(copy)
+
+    for half in range(UNITS):
+        forward(level, half)
     for load in weight_loads:
         load.wait()
     for load in state_loads + big_loads:
         load.start()
-
-    pl.semaphore_wait(barrier, total - 1)
-
-    nearer = jnp.minimum(level, depth - 1 - level)
-
-    def nearest(k):
-        step = (k + 1) // 2 if k % 2 else -(k // 2)
-        beyond = jnp.where(2 * level < depth - 1, k - nearer, nearer - k)
-        return level + jnp.where(k <= 2 * nearer, step, beyond)
-
-    order = [level] + [nearest(k) for k in range(1, depth)]
-
-    def along_z(to, source, slot):
-        return remote(held.at[column, slot], held.at[column, slot], device(to, column), z_send.at[to], z_recv.at[source])
-
-    for to in order[1:]:
-        along_z(to, level, level).start()
-
-    sent = []
-
-    def forward(slot):
-        block = held.at[column, slot]
-        for axis, target in ((0, along_y), (1, along_x)):
-            copy = remote(block, block, target, near_send.at[axis, slot], near_recv.at[axis, slot])
-            copy.start()
-            sent.append(copy)
-
-    def relay(slot):
-        for axis, (of_column, target, part) in enumerate(
-            ((column_y, along_x, slice(0, cut)), (column_x, along_y, slice(cut, model)))
-        ):
-            block = held.at[of_column, slot]
-            remote(block, block, along_y, near_send.at[axis, slot], near_recv.at[axis, slot]).wait_recv()
-            half = block.at[:, part]
-            copy = remote(half, half, target, half_send.at[axis, slot], half_recv.at[axis, slot])
-            copy.start()
-            sent.append(copy)
-
-    forward(level)
     swap = remote(weight.at[core], weight.at[core], mate, mate_send, mate_recv)
     swap.start()
     for load in loads[2:]:
@@ -251,20 +277,24 @@
         place[piece] = place_matrix(piece, place.shape[1], weight.shape[2])
 
     for before, slot in zip(order, order[1:]):
-        along_z(slot, slot, slot).wait_recv()
-        forward(slot)
-        relay(before)
+        for half in range(UNITS):
+            along_z(level, slot, half).wait_recv()
+            onward(slot, half, lambda copy: copy.start())
+            forward(slot, half)
+            if half % 2:
+                relay(before, half // 2)
     swap.wait_recv()
 
-    def compute(of_column):
-        rows = held[of_column].astype(F32).reshape(depth * tokens, model).astype(BF16)
+    def compute(of_column, slots):
+        rows = jnp.concatenate([held[of_column, slot].astype(F32) for slot in slots], axis=0).astype(BF16)
         both = weight[...]
         width = both.shape[2]
         if width % 16:
             both = both.astype(F32)
         both = both.reshape(CORES * ROLES * width, model).astype(BF16)
         result = lax.dot_general(rows, both, (((1,), (1,)), ((), ())), preferred_element_type=F32)
-        cols[of_column] = result.reshape(depth, tokens, result.shape[-1]).astype(BF16)
+        for i, slot in enumerate(slots):
+            cols[of_column, slot] = result[i * tokens : (i + 1) * tokens].astype(BF16)
 
     def handed(of_level, of_column):
         to_chip = of_level * COLUMNS + of_column
@@ -274,26 +304,30 @@
             out_send.at[number], out_recv.at[number],
         )
 
-    def give(of_column):
-        for to in order:
+    def give(of_column, slots):
+        for to in slots:
             if of_column is column and to is level:
                 land[chip // pieces, lax.rem(chip, pieces)] = cols[column, level]
             else:
                 handed(to, of_column).start()
 
-    compute(column)
-    relay(order[-1])
-    give(column)
-    compute(column_y)
-    give(column_y)
-    compute(column_x)
-    give(column_x)
-    for slot in order:
-        for axis, part in ((0, slice(0, cut)), (1, slice(cut, model))):
-            half = held.at[far, slot].at[:, part]
-            remote(half, half, along_x, half_send.at[axis, slot], half_recv.at[axis, slot]).wait_recv()
-    compute(far)
-    give(far)
+    compute(column, order)
+    give(column, order)
+    for turn in range(turns):
+        relay(order[-1], turn)
+    for axis, of_column in ((0, column_y), (1, column_x)):
+        for slot in order:
+            for turn in range(turns):
+                near(axis, of_column, slot, (1 - axis) * turns + turn, along_x).wait_recv()
+        compute(of_column, order)
+        give(of_column, order)
+    for slots in (order[:-1], order[-1:]):
+        for slot in slots:
+            for unit in range(UNITS):
+                block = held.at[far, slot].at[:, halves[unit]]
+                remote(block, block, along_x, half_send.at[slot, unit], half_recv.at[slot, unit]).wait_recv()
+        compute(far, slots)
+        give(far, slots)
 
     def finish(number, carry):
         to_chip = lax.rem(chip + number, chips)
@@ -335,10 +369,9 @@
     added = head_sum(scaled_key * receptance)
     unit_ref[...] = unit_key
     query_ref[...] = decay * receptance
-    value_out[...] = values
-    decay_out[...] = decay
-    removal_out[...] = removal
-    scaled_out[...] = scaled_key
+    decay_ref[...] = decay
+    removal_ref[...] = removal
+    scaled_ref[...] = scaled_key
 
     recalled = jnp.zeros((rows_all, LANES), F32)
     kept = jnp.zeros((rows_all, LANES), F32)
@@ -350,7 +383,7 @@
         recalled = recalled + dot((block * wide_key).astype(BF16), pick)
         wide_query = jnp.concatenate([query_ref[...]] * (span // LANES), axis=1)
         kept = kept + dot((block * wide_query).astype(BF16), pick)
-    recalled_out[...] = recalled
+    recalled_ref[...] = recalled
     values = role_ref[2]
     read = kept - recalled * removed + values * added
     centered = read - head_sum(read) * (1.0 / HEAD_SIZE)
@@ -387,11 +420,22 @@
         number = lax.rem(to - me + total, total)
         return remote(output.at[to], returned.at[me], to, back_send.at[number], back_recv.at[number])
 
-    def launch(number, carry):
-        go(number).start()
-        return carry
-
-    lax.fori_loop(1, total, launch, 0)
+    place_in_plane = lax.rem(me, PLANE)
+
+    def launch(of_level):
+        def one(i, carry):
+            to = of_level * PLANE + lax.rem(place_in_plane + i, PLANE)
+
+            @pl.when(to != me)
+            def _():
+                go(lax.rem(to - me + total, total)).start()
+
+            return carry
+
+        lax.fori_loop(0, PLANE, one, 0)
+
+    for of_level in order[::-1]:
+        launch(of_level)
     served[me] = out_rows[me]
     for load in big_loads[1:4]:
         load.wait()
@@ -400,8 +444,25 @@
     for load in big_loads[4:]:
         load.wait()
 
-    for d in range(depth):
-        first = lax.rem(level + depth - d, depth) * PLANE
+    own_lane = lax.broadcasted_iota(jnp.int32, (rows_all, LANES), 1) < HEAD_SIZE
+    high, low = split(recalled_ref[...])
+    both = jnp.where(own_lane, high.astype(F32), low.astype(F32)).astype(BF16)
+    alone = jnp.where(own_lane, role_ref[2], 0.0).astype(BF16)
+    stacked = jnp.concatenate([both, alone], axis=0)
+    step = 4 * HEAD_SIZE
+
+    def twice(ref):
+        return jnp.concatenate([ref[...]] * (step // LANES), axis=1)
+
+    for first in range(0, state.shape[2], step):
+        spread = dot(stacked, spread_matrix(first // HEAD_SIZE, step))
+        block = state[:, :, first : first + step].reshape(rows_all, step)
+        new = block * twice(decay_ref) - spread[:rows_all] * twice(removal_ref)
+        new = new + spread[rows_all:] * twice(scaled_ref)
+        state[:, :, first : first + step] = new.reshape(tokens, HEAD_COUNT, step)
+
+    for of_level in order[::-1]:
+        first = of_level * PLANE
 
         def arrive(i, carry):
             source = first + i
@@ -440,8 +501,10 @@
     routed = dot(coef_ref[...], returned[...].reshape(total * CAP, model))
     hidden_out[...] = (middle_ref[...] + (routed[:tokens] + routed[tokens:])).astype(BF16)
 
-    for to in order[1:]:
-        along_z(to, level, level).wait_send()
+    each_way(lambda copy: copy.wait_send())
+    for slot in order[1:]:
+        for half in range(UNITS):
+            onward(slot, half, lambda copy: copy.wait_send())
     for copy in sent:
         copy.wait_send()
     swap.wait_send()
@@ -466,12 +529,11 @@
     vmem = pl.BlockSpec(memory_space=pltpu.VMEM)
     operands = (resid, gain, *weights, routes, routing_weight, *consts, state, out_w, ffn_gain, *experts)
     operands = [pltpu.with_memory_space_constraint(a, pltpu.HBM) for a in operands]
-    lanes = jax.ShapeDtypeStruct((rows_all, LANES), F32)
     return pl.pallas_call(
         functools.partial(layer_kernel, depth),
-        out_shape=(jax.ShapeDtypeStruct((tokens, model), BF16),) + (lanes,) * 5,
+        out_shape=(jax.ShapeDtypeStruct((tokens, model), BF16), jax.ShapeDtypeStruct(state.shape, F32)),
         in_specs=[hbm] * len(operands),
-        out_specs=(vmem,) * 6,
+        out_specs=(vmem,) * 2,
         scratch_shapes=[
             pltpu.VMEM((tokens, model), BF16),
             pltpu.VMEM(gain.shape, BF16),
@@ -483,7 +545,6 @@
             pltpu.VMEM((HEAD_COUNT, pieces, tokens, wide), BF16),
             pltpu.VMEM((4,) + consts[0].shape, F32),
             pltpu.VMEM((4, HEAD_COUNT, LANES), F32),
-            pltpu.VMEM(state.shape, F32),
             pltpu.VMEM(out_w.shape, BF16),
             pltpu.VMEM(gain.shape, BF16),
         ]
@@ -491,9 +552,9 @@
         + [
             pltpu.VMEM((pieces, wide, ROLES * LANES), BF16),
             pltpu.VMEM((ROLES, rows_all, LANES), F32),
-            pltpu.VMEM((rows_all, LANES), F32),
-            pltpu.VMEM((rows_all, LANES), F32),
-            pltpu.VMEM((rows_all, LANES), F32),
+        ]
+        + [pltpu.VMEM((rows_all, LANES), F32)] * 7
+        + [
             pltpu.VMEM((tokens, slots), F32),
             pltpu.VMEM((2 * tokens, slots), BF16),
             pltpu.VMEM((tokens, model), F32),
@@ -502,70 +563,46 @@
         + [pltpu.VMEM((ep_size, CAP, model), BF16)] * 4
         + [
             dma((9,)), dma((ROLES,)), dma((PARTS,)), dma((7,)),
-            dma((depth,)), dma((depth,)),
-            dma((2, depth)), dma((2, depth)),
-            dma((2, depth)), dma((2, depth)),
+            dma((2, depth, UNITS)), dma((depth, UNITS)),
+            dma((2, depth, UNITS)), dma((2, depth, UNITS)),
+            dma((depth, UNITS)), dma((depth, UNITS)),
             dma, dma,
             dma((chips,)), dma((chips,)),
         ]
         + [dma((ep_size,))] * 4,
         compiler_params=pltpu.CompilerParams(
-            has_side_effects=True, collective_id=0, vmem_limit_bytes=52 * 1024 * 1024
+            has_side_effects=True, collective_id=0, vmem_limit_bytes=46 * 1024 * 1024
         ),
         cost_estimate=pl.CostEstimate(flops=30_000_000_000, bytes_accessed=100_000_000, transcendentals=0),
     )(*operands)
 
 
-def update_kernel(
-    state, recalled, value, decay, removal, scaled, hidden, next_hbm, hidden_hbm, held, next_sem, hidden_sem
-):
-    copy = pltpu.make_async_copy(hidden, hidden_hbm, hidden_sem)
-    copy.start()
-    group, heads, columns = state.shape
-    rows_all = group * heads
-    span = columns // PARTS
-    step = 4 * HEAD_SIZE
-    lane = lax.broadcasted_iota(jnp.int32, (rows_all, LANES), 1)
-    high, low = split(recalled[...])
-    both = jnp.where(lane < HEAD_SIZE, high.astype(F32), low.astype(F32)).astype(BF16)
-    alone = jnp.where(lane < HEAD_SIZE, value[...], 0.0).astype(BF16)
-    stacked = jnp.concatenate([both, alone], axis=0)
-
-    def twice(ref):
-        return jnp.concatenate([ref[...]] * (step // LANES), axis=1)
-
-    copies = []
-    for part in range(PARTS):
-        for first in range(part * span, (part + 1) * span, step):
-            spread = dot(stacked, spread_matrix(first // HEAD_SIZE, step))
-            block = state[:, :, first : first + step].reshape(rows_all, step)
-            new = block * twice(decay) - spread[:rows_all] * twice(removal) + spread[rows_all:] * twice(scaled)
-            held[:, :, first : first + step] = new.reshape(group, heads, step)
-        here = pl.ds(part * span, span)
-        out = pltpu.make_async_copy(held.at[:, :, here], next_hbm.at[:, :, here], next_sem.at[part])
-        out.start()
-        copies.append(out)
-    for out in copies:
-        out.wait()
-    copy.wait()
-
-
-def update(state, recalled, value, decay, removal, scaled, hidden):
+def store_kernel(state, hidden, next_hbm, hidden_hbm, next_sem, hidden_sem):
+    parts = next_sem.shape[0]
+    group = state.shape[0] // parts
+    copies = [pltpu.make_async_copy(hidden, hidden_hbm, hidden_sem)]
+    for part in range(parts):
+        here = pl.ds(part * group, group)
+        copies.append(pltpu.make_async_copy(state.at[here], next_hbm.at[here], next_sem.at[part]))
+    for copy in copies:
+        copy.start()
+    for copy in copies:
+        copy.wait()
+
+
+def store(state, hidden):
     vmem = pl.BlockSpec(memory_space=pltpu.VMEM)
     hbm = pl.BlockSpec(memory_space=pltpu.HBM)
     dma = pltpu.SemaphoreType.DMA
     return pl.pallas_call(
-        update_kernel,
-        out_shape=(
-            jax.ShapeDtypeStruct(state.shape, F32),
-            jax.ShapeDtypeStruct(hidden.shape, BF16),
-        ),
-        in_specs=[vmem] * 7,
+        store_kernel,
+        out_shape=(jax.ShapeDtypeStruct(state.shape, F32), jax.ShapeDtypeStruct(hidden.shape, BF16)),
+        in_specs=[vmem] * 2,
         out_specs=(hbm, hbm),
-        scratch_shapes=[pltpu.VMEM(state.shape, F32), dma((PARTS,)), dma],
-        compiler_params=pltpu.CompilerParams(vmem_limit_bytes=20 * 1024 * 1024),
+        scratch_shapes=[dma((STORES,)), dma],
+        compiler_params=pltpu.CompilerParams(vmem_limit_bytes=4 * 1024 * 1024),
         cost_estimate=pl.CostEstimate(flops=1_000_000_000, bytes_accessed=20_000_000, transcendentals=0),
-    )(state, recalled, value, decay, removal, scaled, hidden)
+    )(state, hidden)
 
 
 def per_device(
@@ -594,7 +631,7 @@
     common_down_weight,
 ):
     ep_size = lax.axis_size("ep")
-    hidden, recalled, value, decay, removal, scaled = layer(
+    hidden, state = layer(
         residual_input,
         attention_norm_gain,
         (
@@ -621,7 +658,7 @@
         ),
         ep_size,
     )
-    next_state, hidden_out = update(previous_state, recalled, value, decay, removal, scaled, hidden)
+    next_state, hidden_out = store(state, hidden)
     return (hidden_out, next_state)
 
 

time: 67.9 us -> 59.4 us (0.87)
  the two profiles are of different devices: /device:TPU:0 before, /device:TPU:23 now
where the time goes in v2:
time: 59.4 us; the launch traced here: 59.2 us
  Pallas kernels  58.6 us (99%)
  between operations  0.65 us (1%)
    pallas_call x1, Pallas kernels, layer(): pl.pallas_call(functools.partial(layer_kernel, depth), out_shape=(jax.Sha...  55.8 us
    pallas_call x1, Pallas kernels, store(): pl.pallas_call(store_kernel, out_shape=(jax.ShapeDtypeStruct(state.shape,...  2.78 us

profile of v2, /device:TPU:23, one launch (start us, length us, event | category | flops | bytes accessed | tf_op | source)
XLA Modules:
  0.0 59.2 jit_solution(12177695130072758082)
XLA Ops:
  0.6 55.8 %shard_map.230 = (bf16[24,2048]{1,0:T(8,128)(2,1)S(1)}, f32[24,16,4096]{2,1,0:T(8,128)S(1)}) custom-call(bf16[24,2048]{1,0:T(8,128)(2,1)} %resid_hbm.1, bf16[16,128]{1,0:T(8,128)(2,1)} %bitcast.28, bf16[32,2048]{1,0:T(8,128)(2,1)} %bitcast.20, bf16[32,2048]{1,0:T(8,128)(2,1)} %bitcast.21, bf16[32,2048]{1,0:T(8,128)(2,1)} %bitcast.22, ...), custom_call_target="tpu_custom_call" | custom-call | flops 30000001024 | bytes 100000000 | tf_op jit(solution)/shard_map/pallas_call | solution.py:532
  56.4 2.8 %shard_map.231 = (f32[24,16,4096]{2,1,0:T(8,128)}, bf16[24,2048]{1,0:T(8,128)(2,1)}) custom-call(f32[24,16,4096]{2,1,0:T(8,128)S(1)} %get-tuple-element.6.state, bf16[24,2048]{1,0:T(8,128)(2,1)S(1)} %get-tuple-element.7.hidden), custom_call_target="tpu_custom_call" | custom-call | flops 1000000000 | bytes 20000000 | tf_op jit(solution)/shard_map/pallas_call | solution.py:597

commit v3 on v2

--- a/solution.py
+++ b/solution.py
@@ -82,6 +82,35 @@
     coef_out[tokens:] = (chosen * low).astype(BF16)
 
 
+def chosen_tables(routes, me, core, depth, tokens, chosen_ref):
+    everyone = routes.shape[1]
+    sources = everyone // tokens
+    slots, length = chosen_ref.shape[1:]
+    iota = lambda shape, axis: lax.broadcasted_iota(jnp.int32, shape, axis)
+    flag = lambda value: value.astype(F32)
+    hit = jnp.zeros((1, everyone), F32)
+    for entry in range(routes.shape[0]):
+        hit = hit + flag(routes[entry : entry + 1] == me)
+    mine = flag(iota((sources, everyone), 1) // tokens == iota((sources, everyone), 0))
+    fold = flag(iota((everyone, tokens), 0) % tokens == iota((everyone, tokens), 1))
+    table = dot((mine * hit).astype(BF16), fold.astype(BF16))
+    before = flag(iota((tokens, tokens), 0) < iota((tokens, tokens), 1))
+    rank = dot(table.astype(BF16), before.astype(BF16))
+    unfold = flag(iota((tokens, length), 1) % tokens == iota((tokens, length), 0)).astype(BF16)
+    spread_hit = dot(table.astype(BF16), unfold)
+    spread_rank = dot(rank.astype(BF16), unfold)
+    for group in range(CORES):
+        of_core = core if group == 0 else CORES - 1 - core
+        block = iota((1, length), 1) // tokens
+        source = ((block % depth) * COLUMNS + block // depth) * CORES + of_core
+        here = flag(iota((sources, length), 0) == source)
+        hits = jnp.sum(here * spread_hit, axis=0, keepdims=True)
+        ranks = jnp.sum(here * spread_rank, axis=0, keepdims=True)
+        row = iota((slots, length), 0)
+        chosen = flag(row // CAP == source) * hits * flag(flag(row % CAP) == ranks)
+        chosen_ref[group] = chosen.astype(BF16)
+
+
 def place_matrix(piece, rows, width):
     lane = lax.broadcasted_iota(jnp.int32, (1, ROLES * LANES), 1)
     inner = lane % HEAD_SIZE - piece * CORES * width
@@ -119,12 +148,12 @@
     resid_hbm, gain_hbm, w0, w1, w2, w3, w4, w5, routes_hbm, rweight_hbm,
     const0, const1, const2, const3, state_hbm, out_w_hbm, ffn_gain_hbm, g0, g1, g2, g3, g4, g5,
     hidden_out, state,
-    resid, gain, weight, routes, rweight, held, cols, land,
+    gain, weight, routes, rweight, held, mates, cols, land,
     raw, consts, out_w, ffn_gain, b0, b1, b2, b3, b4, b5,
-    place, role_ref, unit_ref, query_ref, mixed_ref, recalled_ref, decay_ref, removal_ref, scaled_ref, select_ref, coef_ref,
+    place, role_ref, unit_ref, query_ref, mixed_ref, recalled_ref, decay_ref, removal_ref, scaled_ref, select_ref, coef_ref, chosen_ref, base_ref,
     middle_ref, normed_ref, out_rows, served, output, returned,
     load_sem, weight_sem, state_sem, big_sem,
-    z_send, z_recv, near_send, near_recv, half_send, half_recv, mate_send, mate_recv,
+    z_send, z_recv, near_send, near_recv, half_send, half_recv, mate_send, mate_recv, exchange_send, exchange_recv,
     out_send, out_recv, go_send, go_recv, back_send, back_recv,
 ):
     total = depth * PLANE
@@ -156,7 +185,9 @@
         pltpu.make_async_copy(source, target, load_sem.at[i])
         for i, (source, target) in enumerate(
             (
-                (resid_hbm, resid), (gain_hbm, gain), (routes_hbm, routes), (rweight_hbm, rweight),
+                (resid_hbm.at[:, pl.ds(0, cut)], held.at[column, level, 0]),
+                (resid_hbm.at[:, pl.ds(cut, cut)], held.at[column, level, 1]),
+                (gain_hbm, gain), (routes_hbm, routes), (rweight_hbm, rweight),
                 (const0, raw.at[0]), (const1, raw.at[1]), (const2, raw.at[2]), (const3, raw.at[3]),
                 (ffn_gain_hbm, ffn_gain),
             )
@@ -196,7 +227,6 @@
 
     loads[0].wait()
     loads[1].wait()
-    held[column, level] = rms_norm(resid[...].astype(F32), gain_row(gain[...]))
     pl.semaphore_wait(barrier, total - 1)
 
     nearer = jnp.minimum(level, depth - 1 - level)
@@ -208,11 +238,10 @@
 
     order = [level] + [nearest(k) for k in range(1, depth)]
 
-    halves = [slice(i * cut, (i + 1) * cut) for i in range(UNITS)]
     turns = UNITS // 2
 
     def along_z(to, slot, half):
-        block = held.at[column, slot].at[:, halves[half]]
+        block = held.at[column, slot, half]
         downward = jnp.where(to > level, 0, 1)
         return remote(
             block, block, device(to, column), z_send.at[downward, slot, half], z_recv.at[slot, half]
@@ -237,12 +266,12 @@
     sent = []
 
     def near(axis, of_column, slot, half, target):
-        block = held.at[of_column, slot].at[:, halves[half]]
+        block = held.at[of_column, slot, half]
         return remote(block, block, target, near_send.at[axis, slot, half], near_recv.at[axis, slot, half])
 
     def forward(slot, half):
         for axis, target in ((0, along_y), (1, along_x)):
-            copy = near(axis, column, slot, half, target)
+            copy = near(axis, column, slot, half if axis == 0 else 1 - half, target)
             copy.start()
             sent.append(copy)
 
@@ -250,7 +279,7 @@
         for axis, (of_column, target) in enumerate(((column_y, along_x), (column_x, along_y))):
             unit = axis * turns + turn
             near(axis, of_column, slot, unit, target).wait_recv()
-            block = held.at[of_column, slot].at[:, halves[unit]]
+            block = held.at[of_column, slot, unit]
             copy = remote(block, block, target, half_send.at[slot, unit], half_recv.at[slot, unit])
             copy.start()
             sent.append(copy)
@@ -266,6 +295,7 @@
     for load in loads[2:]:
         load.wait()
     route_tables(routes[...], rweight[...], me, tokens, select_ref, coef_ref)
+    chosen_tables(routes[...], me, core, depth, tokens, chosen_ref)
     for number in range(4):
         pair = raw[number]
         turned = pltpu.roll(pair, HEAD_SIZE, 1)
@@ -280,13 +310,18 @@
         for half in range(UNITS):
             along_z(level, slot, half).wait_recv()
             onward(slot, half, lambda copy: copy.start())
-            forward(slot, half)
             if half % 2:
+                forward(slot, 0)
+                forward(slot, 1)
                 relay(before, half // 2)
     swap.wait_recv()
 
     def compute(of_column, slots):
-        rows = jnp.concatenate([held[of_column, slot].astype(F32) for slot in slots], axis=0).astype(BF16)
+        sides = [
+            jnp.concatenate([held[of_column, slot, half].astype(F32) for slot in slots], axis=0)
+            for half in range(UNITS)
+        ]
+        rows = rms_norm(jnp.concatenate(sides, axis=1), gain_row(gain[...]))
         both = weight[...]
         width = both.shape[2]
         if width % 16:
@@ -321,11 +356,14 @@
                 near(axis, of_column, slot, (1 - axis) * turns + turn, along_x).wait_recv()
         compute(of_column, order)
         give(of_column, order)
+    exchange = remote(held, mates, mate, exchange_send, exchange_recv)
     for slots in (order[:-1], order[-1:]):
         for slot in slots:
             for unit in range(UNITS):
-                block = held.at[far, slot].at[:, halves[unit]]
+                block = held.at[far, slot, unit]
                 remote(block, block, along_x, half_send.at[slot, unit], half_recv.at[slot, unit]).wait_recv()
+        if slots[-1] is order[-1]:
+            exchange.start()
         compute(far, slots)
         give(far, slots)
 
@@ -401,14 +439,8 @@
             part = jnp.where(lane < other * HEAD_SIZE, part, rest)
         parts.append(part.astype(BF16))
     mixed = jnp.concatenate(parts, axis=1)
-    big_loads[0].wait()
-    attended = dot(mixed, out_w[...]).astype(BF16).astype(F32)
-    middle = resid[...].astype(F32) + attended
-    middle_ref[...] = middle
-    normed = rms_norm(middle, gain_row(ffn_gain[...]))
-    normed_ref[...] = normed
     picked = lax.dot_general(
-        select_ref[...].astype(BF16), normed, (((0,), (0,)), ((), ())), preferred_element_type=F32
+        select_ref[...].astype(BF16), mixed, (((0,), (0,)), ((), ())), preferred_element_type=F32
     )
     out_rows[...] = picked.reshape(out_rows.shape).astype(BF16)
 
@@ -437,6 +469,19 @@
     for of_level in order[::-1]:
         launch(of_level)
     served[me] = out_rows[me]
+    big_loads[0].wait()
+    attended = dot(mixed, out_w[...]).astype(BF16).astype(F32)
+    own_rows = jnp.concatenate([held[column, level, half] for half in range(UNITS)], axis=1)
+    middle = own_rows.astype(F32) + attended
+    middle_ref[...] = middle
+    normed_ref[...] = rms_norm(middle, gain_row(ffn_gain[...]))
+    exchange.wait_recv()
+    for half in range(UNITS):
+        base = jnp.zeros((total * CAP, cut), F32)
+        for group, source in ((0, held), (1, mates)):
+            rows = source[:, :, half].astype(F32).reshape(chips * tokens, cut).astype(BF16)
+            base = base + dot(chosen_ref[group], rows)
+        base_ref[:, half * cut : (half + 1) * cut] = base.astype(BF16)
     for load in big_loads[1:4]:
         load.wait()
     shared = expert_mlp(normed_ref[...], b0[...], b1[...], b2[...])
@@ -444,6 +489,36 @@
     for load in big_loads[4:]:
         load.wait()
 
+    for of_level in order[::-1]:
+        first = of_level * PLANE
+
+        def arrive(i, carry):
+            source = first + i
+
+            @pl.when(source != me)
+            def _():
+                go(lax.rem(me - source + total, total)).wait_recv()
+
+            return carry
+
+        lax.fori_loop(0, PLANE, arrive, 0)
+        rows = served[pl.ds(first, PLANE)].reshape(PLANE * CAP, served.shape[2])
+        projected = dot(rows, out_w[...]).astype(BF16).astype(F32)
+        below = base_ref[pl.ds(pl.multiple_of(first * CAP, PLANE * CAP), PLANE * CAP), :]
+        rows = rms_norm(below.astype(F32) + projected, gain_row(ffn_gain[...]))
+        result = expert_mlp(rows, b3[...], b4[...], b5[...])
+        output[pl.ds(first, PLANE)] = result.reshape(PLANE, CAP, model)
+
+        def give_back(i, carry):
+            source = first + i
+
+            @pl.when(source != me)
+            def _():
+                back(source).start()
+
+            return carry
+
+        lax.fori_loop(0, PLANE, give_back, 0)
     own_lane = lax.broadcasted_iota(jnp.int32, (rows_all, LANES), 1) < HEAD_SIZE
     high, low = split(recalled_ref[...])
     both = jnp.where(own_lane, high.astype(F32), low.astype(F32)).astype(BF16)
@@ -461,33 +536,6 @@
         new = new + spread[rows_all:] * twice(scaled_ref)
         state[:, :, first : first + step] = new.reshape(tokens, HEAD_COUNT, step)
 
-    for of_level in order[::-1]:
-        first = of_level * PLANE
-
-        def arrive(i, carry):
-            source = first + i
-
-            @pl.when(source != me)
-            def _():
-                go(lax.rem(me - source + total, total)).wait_recv()
-
-            return carry
-
-        lax.fori_loop(0, PLANE, arrive, 0)
-        rows = served[pl.ds(first, PLANE)].reshape(PLANE * CAP, model)
-        result = expert_mlp(rows, b3[...], b4[...], b5[...])
-        output[pl.ds(first, PLANE)] = result.reshape(PLANE, CAP, model)
-
-        def give_back(i, carry):
-            source = first + i
-
-            @pl.when(source != me)
-            def _():
-                back(source).start()
-
-            return carry
-
-        lax.fori_loop(0, PLANE, give_back, 0)
     returned[me] = output[me]
 
     def ended(number, carry):
@@ -508,6 +556,7 @@
     for copy in sent:
         copy.wait_send()
     swap.wait_send()
+    exchange.wait_send()
 
 
 def layer(resid, gain, weights, routes, routing_weight, consts, state, out_w, ffn_gain, experts, ep_size):
@@ -535,12 +584,12 @@
         in_specs=[hbm] * len(operands),
         out_specs=(vmem,) * 2,
         scratch_shapes=[
-            pltpu.VMEM((tokens, model), BF16),
             pltpu.VMEM(gain.shape, BF16),
             pltpu.VMEM((CORES, ROLES, width, model), BF16),
             pltpu.VMEM(routes.shape, jnp.int32),
             pltpu.VMEM(routes.shape, F32),
-            pltpu.VMEM((COLUMNS, depth, tokens, model), BF16),
+            pltpu.VMEM((COLUMNS, depth, UNITS, tokens, model // UNITS), BF16),
+            pltpu.VMEM((COLUMNS, depth, UNITS, tokens, model // UNITS), BF16),
             pltpu.VMEM((COLUMNS, depth, tokens, wide), BF16),
             pltpu.VMEM((HEAD_COUNT, pieces, tokens, wide), BF16),
             pltpu.VMEM((4,) + consts[0].shape, F32),
@@ -557,16 +606,19 @@
         + [
             pltpu.VMEM((tokens, slots), F32),
             pltpu.VMEM((2 * tokens, slots), BF16),
+            pltpu.VMEM((CORES, slots, chips * tokens), BF16),
+            pltpu.VMEM((slots, model), BF16),
             pltpu.VMEM((tokens, model), F32),
             pltpu.VMEM((tokens, model), BF16),
         ]
-        + [pltpu.VMEM((ep_size, CAP, model), BF16)] * 4
+        + [pltpu.VMEM((ep_size, CAP, out_w.shape[0]), BF16)] * 2
+        + [pltpu.VMEM((ep_size, CAP, model), BF16)] * 2
         + [
-            dma((9,)), dma((ROLES,)), dma((PARTS,)), dma((7,)),
+            dma((10,)), dma((ROLES,)), dma((PARTS,)), dma((7,)),
             dma((2, depth, UNITS)), dma((depth, UNITS)),
             dma((2, depth, UNITS)), dma((2, depth, UNITS)),
             dma((depth, UNITS)), dma((depth, UNITS)),
-            dma, dma,
+            dma, dma, dma, dma,
             dma((chips,)), dma((chips,)),
         ]
         + [dma((ep_size,))] * 4,

time: 59.4 us -> 58.6 us (0.987)
  the two profiles are of different devices: /device:TPU:23 before, /device:TPU:0 now
where the time goes in v3:
time: 58.6 us; the launch traced here: 58 us
  Pallas kernels  57.2 us (98%)
  between operations  0.81 us (1%)
    pallas_call x1, Pallas kernels, layer(): pl.pallas_call(functools.partial(layer_kernel, depth), out_shape=(jax.Sha...  54.4 us
    pallas_call x1, Pallas kernels, store(): pl.pallas_call(store_kernel, out_shape=(jax.ShapeDtypeStruct(state.shape,...  2.78 us

profile of v3, /device:TPU:0, one launch (start us, length us, event | category | flops | bytes accessed | tf_op | source)
XLA Modules:
  0.0 58.0 jit_solution(4702114447724611588)
XLA Ops:
  0.6 54.4 %shard_map.230 = (bf16[24,2048]{1,0:T(8,128)(2,1)S(1)}, f32[24,16,4096]{2,1,0:T(8,128)S(1)}) custom-call(bf16[24,2048]{1,0:T(8,128)(2,1)} %resid_hbm.1, bf16[16,128]{1,0:T(8,128)(2,1)} %bitcast.28, bf16[32,2048]{1,0:T(8,128)(2,1)} %bitcast.20, bf16[32,2048]{1,0:T(8,128)(2,1)} %bitcast.21, bf16[32,2048]{1,0:T(8,128)(2,1)} %bitcast.22, ...), custom_call_target="tpu_custom_call" | custom-call | flops 30000001024 | bytes 100000000 | tf_op jit(solution)/shard_map/pallas_call | solution.py:581
  55.0 2.8 %shard_map.231 = (f32[24,16,4096]{2,1,0:T(8,128)}, bf16[24,2048]{1,0:T(8,128)(2,1)}) custom-call(f32[24,16,4096]{2,1,0:T(8,128)S(1)} %get-tuple-element.6.state, bf16[24,2048]{1,0:T(8,128)(2,1)S(1)} %get-tuple-element.7.hidden), custom_call_target="tpu_custom_call" | custom-call | flops 1000000000 | bytes 20000000 | tf_op jit(solution)/shard_map/pallas_call | solution.py:649

commit v4 on v3

--- a/solution.py
+++ b/solution.py
@@ -362,8 +362,6 @@
             for unit in range(UNITS):
                 block = held.at[far, slot, unit]
                 remote(block, block, along_x, half_send.at[slot, unit], half_recv.at[slot, unit]).wait_recv()
-        if slots[-1] is order[-1]:
-            exchange.start()
         compute(far, slots)
         give(far, slots)
 
@@ -377,6 +375,7 @@
         return carry
 
     lax.fori_loop(1, chips, finish, 0)
+    exchange.start()
 
     spread_out = jnp.zeros((rows_all, ROLES * LANES), F32)
     for piece in range(pieces):

time: 58.6 us -> 58.6 us (level)
  no operation moved by 1% of the time
where the time goes in v4:
time: 58.6 us; the launch traced here: 58 us
  Pallas kernels  57.2 us (98%)
  between operations  0.81 us (1%)
    pallas_call x1, Pallas kernels, layer(): pl.pallas_call(functools.partial(layer_kernel, depth), out_shape=(jax.Sha...  54.4 us
    pallas_call x1, Pallas kernels, store(): pl.pallas_call(store_kernel, out_shape=(jax.ShapeDtypeStruct(state.shape,...  2.78 us

profile of v4, /device:TPU:0, one launch (start us, length us, event | category | flops | bytes accessed | tf_op | source)
XLA Modules:
  0.0 58.0 jit_solution(8159392554844108483)
XLA Ops:
  0.6 54.4 %shard_map.230 = (bf16[24,2048]{1,0:T(8,128)(2,1)S(1)}, f32[24,16,4096]{2,1,0:T(8,128)S(1)}) custom-call(bf16[24,2048]{1,0:T(8,128)(2,1)} %resid_hbm.1, bf16[16,128]{1,0:T(8,128)(2,1)} %bitcast.28, bf16[32,2048]{1,0:T(8,128)(2,1)} %bitcast.20, bf16[32,2048]{1,0:T(8,128)(2,1)} %bitcast.21, bf16[32,2048]{1,0:T(8,128)(2,1)} %bitcast.22, ...), custom_call_target="tpu_custom_call" | custom-call | flops 30000001024 | bytes 100000000 | tf_op jit(solution)/shard_map/pallas_call | solution.py:580
  55.0 2.8 %shard_map.231 = (f32[24,16,4096]{2,1,0:T(8,128)}, bf16[24,2048]{1,0:T(8,128)(2,1)}) custom-call(f32[24,16,4096]{2,1,0:T(8,128)S(1)} %get-tuple-element.6.state, bf16[24,2048]{1,0:T(8,128)(2,1)S(1)} %get-tuple-element.7.hidden), custom_call_target="tpu_custom_call" | custom-call | flops 1000000000 | bytes 20000000 | tf_op jit(solution)/shard_map/pallas_call | solution.py:648
